TPU v7x, 32 devices: a whole 2x2x4 slice. The times are simulated.
32 devices in a mesh: fs: 16 (over z, y, x), tp: 2 (over core).
Axes of the slice: x: 2, y: 2, z: 4, core: 2. Of those that a mesh axis runs over, the one named last changes fastest.
Arguments:
- tokens: bfloat16 [12288, 2048], P('fs'), may hold values from -6 to 6
- norm_gain: float32 [2048], replicated, may hold values from 0.1 to 1.9
- gate_weight: float32 [2048, 5120], P('fs', 'tp'), may hold values from -0.125 to 0.125
- value_weight: float32 [2048, 5120], P('fs', 'tp'), may hold values from -0.125 to 0.125
- gate_scale: float32 [5120], P('tp'), may hold values from 0.3 to 3
- value_scale: float32 [5120], P('tp'), may hold values from 0.3 to 3
- gate_kernel: float32 [3, 5120], P(None, 'tp'), may hold values from -3.5 to 3.5
- value_kernel: float32 [3, 5120], P(None, 'tp'), may hold values from -3.5 to 3.5
- gate_bias: float32 [5120], P('tp'), may hold values from -3 to 3
- value_bias: float32 [5120], P('tp'), may hold values from -3 to 3
- down_weight: float32 [5120, 2048], P('tp', 'fs'), may hold values from -0.078125 to 0.078125
- down_scale: float32 [2048], P('tp'), may hold values from 0.3 to 3
Outputs:
- mixed: bfloat16 [12288, 2048], P('fs', 'tp')
All inputs are finite; a program needn't handle non-finite values.
Results may differ from a plain program's by a relative error of at most 0.014.
Values may be sent and summed in bfloat16 or wider, within the bound.
A program may use at most 128 MiB of HBM per device.

v0:
```python
import functools
import math

import jax
import jax.numpy as jnp
from jax import lax
from jax.experimental import pallas as pl
from jax.experimental.pallas import tpu as pltpu
from jax.sharding import PartitionSpec as P

epsilon = 1e-06


def from_behind(value, axis, steps):
    count = lax.axis_size(axis)
    leading, last = (max(0, -steps), min(count, count - steps))
    return lax.ppermute(value, axis, [(source, source + steps) for source in range(leading, last)])


def normalize(tokens, norm_gain):
    values = tokens.astype(jnp.float32)
    scaled = values * lax.rsqrt(jnp.mean(values * values, axis=1, keepdims=True) + epsilon)
    return (scaled * norm_gain[None, :]).astype(jnp.bfloat16)


def causal_mix(current, previous, kernel, tap_bias):
    row_count = current.shape[0]
    joined = jnp.concatenate([previous, current], axis=0).astype(jnp.float32)
    summed_taps = tap_bias[None, :] + kernel[2][None, :] * joined[2:]
    for back_by in (1, 2):
        summed_taps = (
            summed_taps
            + kernel[2 - back_by][None, :] * joined[2 - back_by : 2 - back_by + row_count]
        )
    return summed_taps


def body(
    tokens,
    norm_gain,
    gate_weight,
    value_weight,
    gate_scale,
    value_scale,
    gate_kernel,
    value_kernel,
    gate_bias,
    value_bias,
    down_weight,
    down_scale,
):
    normed = normalize(tokens, norm_gain)
    gate_low = gate_weight.astype(jnp.bfloat16)
    value_low = value_weight.astype(jnp.bfloat16)
    down_low = down_weight.astype(jnp.bfloat16)
    row_count = normed.shape[0]
    gate_full, value_full, down_full = (
        lax.all_gather(gate_low, "fs", axis=0, tiled=True),
        lax.all_gather(value_low, "fs", axis=0, tiled=True),
        lax.all_gather(down_low, "fs", axis=1, tiled=True),
    )
    gate_raw = jnp.dot(normed, gate_full, preferred_element_type=jnp.float32)
    value_raw = jnp.dot(normed, value_full, preferred_element_type=jnp.float32)
    gate_pre = (gate_raw * gate_scale[None, :]).astype(jnp.bfloat16)
    value_pre = (value_raw * value_scale[None, :]).astype(jnp.bfloat16)
    previous_gate, previous_value = from_behind(
        (gate_pre[row_count - 2 :], value_pre[row_count - 2 :]), "fs", 1
    )
    gate_conv = causal_mix(gate_pre, previous_gate, gate_kernel, gate_bias)
    value_conv = causal_mix(value_pre, previous_value, value_kernel, value_bias)
    hidden = (jax.nn.gelu(gate_conv, approximate=True) * value_conv).astype(jnp.bfloat16)
    partial_terms = jnp.dot(hidden, down_full, preferred_element_type=jnp.float32)
    summed = lax.psum_scatter(
        partial_terms.astype(jnp.bfloat16), "tp", scatter_dimension=1, tiled=True
    ).astype(jnp.float32)
    return (summed * down_scale[None, :]).astype(jnp.bfloat16)


MESH = pl.DeviceIdType.MESH
GROUP = 4


def fused_kernel(
    depth_planes,
    tok_hbm,
    gate_hbm,
    value_hbm,
    down_hbm,
    gain,
    gate_scale,
    value_scale,
    gate_kernel,
    value_kernel,
    gate_bias,
    value_bias,
    osc,
    out,
    tok,
    up_all,
    down_all,
    hidden,
    stage,
    pair_in,
    peer_in,
    relay_in,
    taps,
    halo_out,
    halo_in,
    par,
    wu,
    wd,
    raw_tok,
    raw_gate,
    raw_value,
    raw_down,
    sem_local,
    sem_plane_send,
    sem_up_recv,
    sem_down_recv,
    sem_up_send,
    sem_down_send,
    sem_tok_send,
    sem_tok_recv,
    sem_tok_pair_send,
    sem_tok_pair_recv,
    sem_halo,
    sem_pair_send,
    sem_pair_recv,
    sem_peer_send,
    sem_peer_recv,
    sem_relay_send,
    sem_relay_recv,
    sem_late_recv,
    sem_late_send,
):
    planes = depth_planes
    half = planes // 2
    me = lax.axis_index("fs")
    core = lax.axis_index("tp")
    z, p = me // GROUP, me % GROUP
    rows_own = raw_tok.shape[0]
    part_rows = rows_own // 2
    piece = wu.shape[1]
    units = hidden.shape[1]
    out_piece = wd.shape[2]
    chunk = GROUP * out_piece
    has_up, has_down = z < planes - 1, z > 0

    def flip(mask):
        px, py = p % 2, p // 2
        if mask & 1:
            px = 1 - px
        if mask & 2:
            py = 1 - py
        return py * 2 + px

    def chip(target):
        return (z * GROUP + target, core)

    others = (1, 2, 3)

    fetches = [
        pltpu.make_async_copy(src, dst, sem_local.at[2 + i])
        for i, (src, dst) in enumerate(
            ((gate_hbm, raw_gate), (value_hbm, raw_value), (down_hbm, raw_down), (tok_hbm, raw_tok))
        )
    ]
    for fetch in fetches:
        fetch.start()

    barrier = pltpu.get_barrier_semaphore()
    for mask in others:
        pl.semaphore_signal(barrier, inc=1, device_id=chip(flip(mask)), device_id_type=MESH)
    pl.semaphore_signal(barrier, inc=1, device_id=(me, 1 - core), device_id_type=MESH)

    @pl.when(has_up)
    def _():
        pl.semaphore_signal(barrier, inc=1, device_id=(me + GROUP, core), device_id_type=MESH)

    @pl.when(has_down)
    def _():
        pl.semaphore_signal(barrier, inc=1, device_id=(me - GROUP, core), device_id_type=MESH)

    blocks = units // 128
    fetches[0].wait()
    fetches[1].wait()
    for m in range(GROUP):
        for j in range(blocks):
            first = (m * blocks + j) * 128
            wu[m, :, j * 256 : j * 256 + 128] = raw_gate[:, first : first + 128].astype(jnp.bfloat16)
            wu[m, :, j * 256 + 128 : j * 256 + 256] = raw_value[:, first : first + 128].astype(jnp.bfloat16)
    fetches[2].wait()
    for m in range(GROUP):
        wd[m] = raw_down[m * units : (m + 1) * units, :].astype(jnp.bfloat16)
    for j in range(blocks):
        src = pl.ds(pl.multiple_of(p * units + j * 128, 128), 128)
        for side, (scale, kernel, tap_bias) in enumerate(
            ((gate_scale, gate_kernel, gate_bias), (value_scale, value_kernel, value_bias))
        ):
            dst = slice(j * 256 + side * 128, j * 256 + side * 128 + 128)
            par[0:1, dst] = scale[0:1, src]
            par[1:4, dst] = kernel[0:3, src]
            par[4:5, dst] = tap_bias[0:1, src]
    pl.semaphore_wait(barrier, 4 + has_up.astype(jnp.int32) + has_down.astype(jnp.int32))

    early = (blocks + 1) // 2 * 256
    columns = up_all.shape[1]

    def up_whole(f):
        return up_all.at[pl.ds(pl.multiple_of(f * piece, piece), piece), :]

    def up_block(f):
        return up_all.at[pl.ds(pl.multiple_of(f * piece, piece), piece), 0:early]

    def late_block(f):
        return up_all.at[pl.ds(pl.multiple_of(f * piece, piece), piece), early:columns]

    def down_block(f):
        return down_all.at[:, pl.ds(pl.multiple_of(f * out_piece, out_piece), out_piece)]

    kinds = (
        (up_block, sem_up_send, sem_up_recv),
        (down_block, sem_down_send, sem_down_recv),
        (late_block, sem_late_send, sem_late_recv),
    )

    def remote(src, dst, send, recv, device):
        return pltpu.make_async_remote_copy(
            src_ref=src, dst_ref=dst, send_sem=send, recv_sem=recv, device_id=device, device_id_type=MESH
        )

    def plane_copy(kind, mask):
        target = flip(mask)
        block, _, recv = kinds[kind]
        src = (wu.at[target, :, 0:early], wd.at[target], wu.at[target, :, early:columns])[kind]
        return remote(src, block(me), sem_plane_send.at[kind, mask], recv.at[me], chip(target))

    def line_copy(kind, direction, f):
        block, send, recv = kinds[kind]
        step = GROUP if direction == 0 else -GROUP
        return remote(block(f), block(f), send.at[direction, f], recv.at[f], (me + step, core))

    def wait_piece(kind, f):
        block, send, recv = kinds[kind]
        remote(block(f), block(f), send.at[0, f], recv.at[f], (me, 1 - core)).wait_recv()

    def forward(kind, direction, f):
        @pl.when(has_up if direction == 0 else has_down)
        def _():
            line_copy(kind, direction, f).start()

    def token_rows(owner, part):
        start = pl.multiple_of(owner * rows_own + part * part_rows, part_rows)
        return tok.at[pl.ds(start, part_rows), :]

    def token_copy(mask):
        here = token_rows(p, core)
        return remote(here, here, sem_tok_send.at[mask], sem_tok_recv.at[mask], chip(flip(mask)))

    quarter = part_rows // 2

    def token_quarter(owner, which):
        start = owner * rows_own + core * part_rows + which * quarter
        return tok.at[pl.ds(pl.multiple_of(start, quarter), quarter), :]

    def token_relay(mask):
        which = mask - 1
        slot = (3, 0)[which]
        here = token_quarter(flip(mask), which)
        return remote(here, here, sem_tok_send.at[slot], sem_tok_recv.at[slot], chip(flip(3 - mask)))

    def token_pair_copy(mask):
        here = token_rows(flip(mask), core)
        return remote(here, here, sem_tok_pair_send.at[mask], sem_tok_pair_recv.at[mask], (me, 1 - core))

    own_up = pltpu.make_async_copy(wu.at[p], up_whole(me), sem_local.at[0])
    own_down = pltpu.make_async_copy(wd.at[p], down_block(me), sem_local.at[1])
    own_up.start()
    own_down.start()
    for kind in (0, 2):
        for mask in others:
            plane_copy(kind, mask).start()
    own_up.wait()
    for direction in (0, 1):
        forward(0, direction, me)

    fetches[3].wait()
    norm_tile = 64

    def norm_step(i, carry):
        first = pl.multiple_of(i * norm_tile, norm_tile)
        values = raw_tok[pl.ds(first, norm_tile), :].astype(jnp.float32)
        scaled = values * lax.rsqrt(jnp.mean(values * values, axis=1, keepdims=True) + epsilon)
        rows = pl.ds(pl.multiple_of(p * rows_own + i * norm_tile, norm_tile), norm_tile)
        tok[rows, :] = (scaled * gain[...]).astype(jnp.bfloat16)
        return carry

    lax.fori_loop(0, rows_own // norm_tile, norm_step, 0)
    own_down.wait()

    def own_plane(kind):
        for mask in others:
            f = z * GROUP + flip(mask)
            wait_piece(kind, f)
            for direction in (0, 1):
                forward(kind, direction, f)

    own_plane(0)
    for mask in (1, 2):
        token_copy(mask).start()
    for mask in others:
        plane_copy(1, mask).start()
    for direction in (0, 1):
        forward(2, direction, me)
    own_plane(2)

    def plane_of(step):
        distance = (step + 1) // 2
        below = step % 2
        return z + distance * (1 - 2 * below), below

    def relay_one(kind, q, below, i):
        f = q * GROUP + i
        wait_piece(kind, f)

        @pl.when((below == 1) & has_up)
        def _():
            line_copy(kind, 0, f).start()

        @pl.when((below == 0) & has_down)
        def _():
            line_copy(kind, 1, f).start()

    def relay(kind, q, below):
        def one(i, carry):
            relay_one(kind, q, below, i)
            return carry

        lax.fori_loop(0, GROUP, one, 0)

    def up_step(step, carry):
        q, below = plane_of(step)

        @pl.when((q >= 0) & (q < planes))
        def _():
            relay(0, q, below)

        return carry

    lax.fori_loop(1, 2 * planes - 3, up_step, 0)

    def token_wait(mask):
        landed = token_rows(flip(mask), core)
        remote(landed, landed, sem_tok_send.at[mask], sem_tok_recv.at[mask], (me, 1 - core)).wait_recv()

    for mask in (1, 2):
        token_wait(mask)
        token_relay(mask).start()
        token_pair_copy(mask).start()

    lax.fori_loop(2 * planes - 3, 2 * planes - 1, up_step, 0)

    def token_pair_wait(mask):
        there = token_rows(flip(mask), 1 - core)
        remote(there, there, sem_tok_pair_send.at[mask], sem_tok_pair_recv.at[mask], (me, 1 - core)).wait_recv()

    for which in (0, 1):
        slot = (3, 0)[which]
        landed = token_quarter(flip(3), which)
        remote(landed, landed, sem_tok_send.at[slot], sem_tok_recv.at[slot], (me, 1 - core)).wait_recv()
    token_pair_copy(3).start()
    for mask in others:
        token_pair_wait(mask)

    all_rows = tok.shape[0]
    tile = taps.shape[0] - 8
    halo_rows = halo_out.shape[0]

    def wide(j):
        return pl.ds(pl.multiple_of(j * 256, 256), 256)

    def halo_step(j, carry):
        raw = jnp.dot(tok[all_rows - halo_rows :, :], up_all[:, wide(j)], preferred_element_type=jnp.float32)
        halo_out[:, wide(j)] = (raw * par[0:1, wide(j)]).astype(jnp.bfloat16)
        return carry

    def halo_copy(part):
        cols = (slice(0, early), slice(early, columns))[part]
        here, there = halo_out.at[:, cols], halo_in.at[:, cols]
        return remote(here, there, sem_halo.at[part], sem_halo.at[2 + part], (me + GROUP, core))

    def halo_part(part, first, last):
        lax.fori_loop(first, last, halo_step, 0)

        @pl.when(has_up)
        def _():
            halo_copy(part).start()

        @pl.when(has_down)
        def _():
            cols = (slice(0, early), slice(early, columns))[part]
            here = halo_in.at[:, cols]
            remote(here, here, sem_halo.at[part], sem_halo.at[2 + part], (me, 1 - core)).wait_recv()

    @pl.when(jnp.logical_not(has_down))
    def _():
        halo_in[...] = jnp.zeros_like(halo_in)

    tiles = all_rows // tile
    slots = (2 * planes - 2) * GROUP
    per_tile = -(-slots // (early // 256 * tiles))

    def late_slot(slot):
        q, below = plane_of(slot // GROUP + 1)

        @pl.when((q >= 0) & (q < planes))
        def _():
            relay_one(2, q, below, slot % GROUP)

    def column_step(j, carry):
        taps[0:8, :] = halo_in[:, wide(j)].astype(jnp.float32)[halo_rows - 8 :, :]

        def row_step(m, inner):
            rows = pl.ds(pl.multiple_of(m * tile, tile), tile)
            raw = jnp.dot(tok[rows, :], up_all[:, wide(j)], preferred_element_type=jnp.float32)
            taps[8:, :] = (raw * par[0:1, wide(j)]).astype(jnp.bfloat16).astype(jnp.float32)
            conv = par[4:5, wide(j)] + par[3:4, wide(j)] * taps[8 : 8 + tile, :]
            conv = conv + par[2:3, wide(j)] * taps[7 : 7 + tile, :]
            conv = conv + par[1:2, wide(j)] * taps[6 : 6 + tile, :]
            g, v = conv[:, :128], conv[:, 128:]
            act = 0.5 * g * (1.0 + jnp.tanh(math.sqrt(2.0 / math.pi) * (g + 0.044715 * (g * g * g))))
            hidden[rows, pl.ds(pl.multiple_of(j * 128, 128), 128)] = (act * v).astype(jnp.bfloat16)
            taps[0:8, :] = taps[tile : tile + 8, :]
            for k in range(per_tile):
                slot = (j * tiles + m) * per_tile + k

                @pl.when((slot < slots) & (j < early // 256))
                def _():
                    late_slot(slot)

            return inner

        return lax.fori_loop(0, tiles, row_step, carry)

    early_blocks = early // 256
    halo_part(0, 0, early_blocks)
    lax.fori_loop(0, early_blocks, column_step, 0)

    for direction in (0, 1):
        forward(1, direction, me)
    own_plane(1)
    if early_blocks < blocks:
        halo_part(1, early_blocks, blocks)
        lax.fori_loop(early_blocks, blocks, column_step, 0)

    def block_rows(owner):
        return pl.ds(pl.multiple_of(owner * rows_own, rows_own), rows_own)

    def pair_copy(q, owner):
        return remote(
            stage.at[q, owner],
            pair_in.at[q % half, owner],
            sem_pair_send.at[q % half, owner],
            sem_pair_recv.at[q % half, owner],
            (me, 1 - core),
        )

    half_rows = rows_own // 2

    def half_of(which):
        return pl.ds(which * half_rows, half_rows)

    def peer_copy(q, mask, which):
        slot = (mask - 1) * 2 + which
        return remote(
            stage.at[q, flip(mask), half_of(which)],
            peer_in.at[q % half, mask - 1, half_of(which)],
            sem_peer_send.at[q % half, slot],
            sem_peer_recv.at[q % half, slot],
            chip(flip(mask)),
        )

    def relay_copy(q, mask):
        return remote(
            stage.at[q, flip(3), half_of(mask - 1)],
            relay_in.at[q % half, mask - 1],
            sem_relay_send.at[q % half, mask - 1],
            sem_relay_recv.at[q % half, mask - 1],
            chip(flip(mask)),
        )

    def down_step(step, carry):
        q, below = plane_of(step)

        @pl.when((q >= 0) & (q < planes))
        def _():
            @pl.when(step > 0)
            def _():
                relay(1, q, below)

            mine = q // half == core
            cols = pl.ds(pl.multiple_of(q * chunk, chunk), chunk)

            def product(owner, inner):
                value = jnp.dot(hidden[block_rows(owner), :], down_all[:, cols], preferred_element_type=jnp.float32)
                stage[q, owner] = value.astype(jnp.bfloat16)

                @pl.when(jnp.logical_not(mine))
                def _():
                    pair_copy(q, owner).start()

                return inner

            lax.fori_loop(0, GROUP, product, 0)

            @pl.when(mine)
            def _():
                def combine(owner):
                    pair_copy(q, owner).wait_recv()
                    both = stage[q, owner].astype(jnp.float32) + pair_in[q % half, owner].astype(jnp.float32)
                    stage[q, owner] = both.astype(jnp.bfloat16)

                combine(flip(3))
                for mask in (1, 2):
                    relay_copy(q, mask).start()
                for mask in (1, 2):
                    combine(flip(mask))
                    peer_copy(q, mask, mask - 1).start()
                combine(p)
                for mask in (1, 2):
                    relay_copy(q, mask).wait_recv()
                    owner = flip(3 - mask)
                    rows = half_of(mask - 1)
                    total = stage[q, owner, rows, :].astype(jnp.float32) + relay_in[q % half, mask - 1].astype(jnp.float32)
                    stage[q, owner, rows, :] = total.astype(jnp.bfloat16)
                    peer_copy(q, 3 - mask, mask - 1).start()

        return carry

    lax.fori_loop(0, 2 * planes - 1, down_step, 0)

    def finish(i, carry):
        q = core * half + i
        total = stage[q, p].astype(jnp.float32)
        for mask in (1, 2):
            for which in (0, 1):
                peer_copy(q, mask, which).wait_recv()
            total = total + peer_in[i, mask - 1].astype(jnp.float32)
        cols = pl.ds(pl.multiple_of(i * chunk, chunk), chunk)
        out[:, cols] = (total * osc[0:1, cols]).astype(jnp.bfloat16)
        return carry

    lax.fori_loop(0, half, finish, 0)

    def drain_out(i, carry):
        for mask in (1, 2):
            relay_copy(core * half + i, mask).wait_send()
            for which in (0, 1):
                peer_copy(core * half + i, mask, which).wait_send()

        def one(owner, inner):
            pair_copy((1 - core) * half + i, owner).wait_send()
            return inner

        return lax.fori_loop(0, GROUP, one, carry)

    lax.fori_loop(0, half, drain_out, 0)
    for mask in (1, 2):
        token_copy(mask).wait_send()
        token_relay(mask).wait_send()
    for mask in others:
        token_pair_copy(mask).wait_send()
        for kind in (0, 1, 2):
            plane_copy(kind, mask).wait_send()

    @pl.when(has_up)
    def _():
        halo_copy(0).wait_send()
        if early < columns:
            halo_copy(1).wait_send()

    def drain_line(f, carry):
        for kind in (0, 1, 2):

            @pl.when(has_up & (f // GROUP <= z))
            def _():
                line_copy(kind, 0, f).wait_send()

            @pl.when(has_down & (f // GROUP >= z))
            def _():
                line_copy(kind, 1, f).wait_send()

        return carry

    lax.fori_loop(0, planes * GROUP, drain_line, 0)


def grouped_body(count, tokens, norm_gain, gate_weight, value_weight, gate_scale, value_scale, gate_kernel, value_kernel, gate_bias, value_bias, down_weight, down_scale):
    planes = count // GROUP
    half = planes // 2
    rows, width = tokens.shape
    piece, local = gate_weight.shape
    out_piece = down_weight.shape[1]
    units = local // GROUP
    chunk = GROUP * out_piece
    tile = rows
    dma = pltpu.SemaphoreType.DMA
    bf16, f32 = jnp.bfloat16, jnp.float32
    vmem = pl.BlockSpec(memory_space=pltpu.VMEM)
    hbm = pl.BlockSpec(memory_space=pl.ANY)
    return pl.pallas_call(
        functools.partial(fused_kernel, planes),
        out_shape=jax.ShapeDtypeStruct((rows, half * chunk), bf16),
        in_specs=[hbm] * 4 + [vmem] * 8,
        out_specs=vmem,
        scratch_shapes=[
            pltpu.VMEM((GROUP * rows, width), bf16),
            pltpu.VMEM((width, 2 * units), bf16),
            pltpu.VMEM((units, width), bf16),
            pltpu.VMEM((GROUP * rows, units), bf16),
            pltpu.VMEM((planes, GROUP, rows, chunk), bf16),
            pltpu.VMEM((half, GROUP, rows, chunk), bf16),
            pltpu.VMEM((half, 2, rows, chunk), bf16),
            pltpu.VMEM((half, 2, rows // 2, chunk), bf16),
            pltpu.VMEM((tile + 8, 256), f32),
            pltpu.VMEM((16, 2 * units), bf16),
            pltpu.VMEM((16, 2 * units), bf16),
            pltpu.VMEM((8, 2 * units), f32),
            pltpu.VMEM((GROUP, piece, 2 * units), bf16),
            pltpu.VMEM((GROUP, units, out_piece), bf16),
            pltpu.VMEM((rows, width), bf16),
            pltpu.VMEM((piece, local), f32),
            pltpu.VMEM((piece, local), f32),
            pltpu.VMEM((local, out_piece), f32),
            dma((6,)),
            dma((3, GROUP)),
            dma((count,)),
            dma((count,)),
            dma((2, count)),
            dma((2, count)),
            dma((GROUP,)),
            dma((GROUP,)),
            dma((GROUP,)),
            dma((GROUP,)),
            dma((4,)),
            dma((half, GROUP)),
            dma((half, GROUP)),
            dma((half, 4)),
            dma((half, 4)),
            dma((half, 2)),
            dma((half, 2)),
            dma((count,)),
            dma((2, count)),
        ],
        compiler_params=pltpu.CompilerParams(
            collective_id=0, has_side_effects=True, vmem_limit_bytes=67043328
        ),
    )(
        tokens,
        gate_weight,
        value_weight,
        down_weight,
        norm_gain[None, :],
        gate_scale[None, :],
        value_scale[None, :],
        gate_kernel,
        value_kernel,
        gate_bias[None, :],
        value_bias[None, :],
        down_scale[None, :],
    )


def solution(mesh):
    count, tp = mesh.shape["fs"], mesh.shape["tp"]

    def whole(*arrays):
        local = arrays[2].shape[1]
        fits = tp == 2 and count % (2 * GROUP) == 0 and local % (GROUP * 128) == 0
        if fits:
            return grouped_body(count, *arrays)
        return body(*arrays)

    return jax.shard_map(
        whole,
        mesh=mesh,
        in_specs=(
            P("fs", None),
            P(),
            P("fs", "tp"),
            P("fs", "tp"),
            P("tp"),
            P("tp"),
            P(None, "tp"),
            P(None, "tp"),
            P("tp"),
            P("tp"),
            P("tp", "fs"),
            P("tp"),
        ),
        out_specs=P("fs", "tp"),
        check_vma=False,
    )
```

profile of v0, /device:TPU:1, one launch (start us, length us, event | category | flops | bytes accessed | tf_op | source)
XLA Modules:
  0.0 218.0 jit_solution(5143176059963249508)
XLA Ops:
  0.0 1.3 broadcast_in_dim.19.gate_scale
  1.3 1.3 broadcast_in_dim.20.value_scale
  2.6 1.3 broadcast_in_dim.21.gate_bias
  3.9 1.3 broadcast_in_dim.22.value_bias
  5.2 210.1 %shard_map.118 = bf16[768,1024]{1,0:T(8,128)(2,1)} custom-call(bf16[768,2048]{1,0:T(8,128)(2,1)} %tok_hbm.1, f32[128,2560]{1,0:T(8,128)} %gate_hbm.1, f32[128,2560]{1,0:T(8,128)} %value_hbm.1, f32[2560,128]{1,0:T(8,128)} %down_hbm.1, f32[1,2048]{1,0:T(1,128)} %bitcast.2, f32[1,2560]{1,0:T(1,128)} %broadcast_in_dim.19.gate_scale, ...), custom_call_target="tpu_custom_call" | custom-call | tf_op jit(solution)/shard_map/pallas_call | solution.py:611
  215.3 2.7 %copy.14 = bf16[768,1024]{1,0:T(8,128)(2,1)} copy(bf16[768,1024]{1,0:T(8,128)(2,1)} %shard_map.118) | data formatting | bytes 3145728
where the time goes:
time: 218 us
  Pallas kernels  210 us (96%)
  local copies, waits for them, and re-layouts  7.91 us (4%)
    pallas_call x1, Pallas kernels, grouped_body(): pl.pallas_call(functools.partial(fused_kernel, planes), out_shape=jax.Sha...  210 us

commit v1 on v0

v1 whole, which is shorter than its diff:
```python
import functools
import math

import jax
import jax.numpy as jnp
from jax import lax
from jax.experimental import pallas as pl
from jax.experimental.pallas import tpu as pltpu
from jax.sharding import PartitionSpec as P

epsilon = 1e-06


def from_behind(value, axis, steps):
    count = lax.axis_size(axis)
    leading, last = (max(0, -steps), min(count, count - steps))
    return lax.ppermute(value, axis, [(source, source + steps) for source in range(leading, last)])


def normalize(tokens, norm_gain):
    values = tokens.astype(jnp.float32)
    scaled = values * lax.rsqrt(jnp.mean(values * values, axis=1, keepdims=True) + epsilon)
    return (scaled * norm_gain[None, :]).astype(jnp.bfloat16)


def causal_mix(current, previous, kernel, tap_bias):
    row_count = current.shape[0]
    joined = jnp.concatenate([previous, current], axis=0).astype(jnp.float32)
    summed_taps = tap_bias[None, :] + kernel[2][None, :] * joined[2:]
    for back_by in (1, 2):
        summed_taps = (
            summed_taps
            + kernel[2 - back_by][None, :] * joined[2 - back_by : 2 - back_by + row_count]
        )
    return summed_taps


def body(
    tokens,
    norm_gain,
    gate_weight,
    value_weight,
    gate_scale,
    value_scale,
    gate_kernel,
    value_kernel,
    gate_bias,
    value_bias,
    down_weight,
    down_scale,
):
    normed = normalize(tokens, norm_gain)
    gate_low = gate_weight.astype(jnp.bfloat16)
    value_low = value_weight.astype(jnp.bfloat16)
    down_low = down_weight.astype(jnp.bfloat16)
    row_count = normed.shape[0]
    gate_full, value_full, down_full = (
        lax.all_gather(gate_low, "fs", axis=0, tiled=True),
        lax.all_gather(value_low, "fs", axis=0, tiled=True),
        lax.all_gather(down_low, "fs", axis=1, tiled=True),
    )
    gate_raw = jnp.dot(normed, gate_full, preferred_element_type=jnp.float32)
    value_raw = jnp.dot(normed, value_full, preferred_element_type=jnp.float32)
    gate_pre = (gate_raw * gate_scale[None, :]).astype(jnp.bfloat16)
    value_pre = (value_raw * value_scale[None, :]).astype(jnp.bfloat16)
    previous_gate, previous_value = from_behind(
        (gate_pre[row_count - 2 :], value_pre[row_count - 2 :]), "fs", 1
    )
    gate_conv = causal_mix(gate_pre, previous_gate, gate_kernel, gate_bias)
    value_conv = causal_mix(value_pre, previous_value, value_kernel, value_bias)
    hidden = (jax.nn.gelu(gate_conv, approximate=True) * value_conv).astype(jnp.bfloat16)
    partial_terms = jnp.dot(hidden, down_full, preferred_element_type=jnp.float32)
    summed = lax.psum_scatter(
        partial_terms.astype(jnp.bfloat16), "tp", scatter_dimension=1, tiled=True
    ).astype(jnp.float32)
    return (summed * down_scale[None, :]).astype(jnp.bfloat16)


MESH = pl.DeviceIdType.MESH
GROUP = 4
EDGE = 16


def fused_kernel(
    depth_planes,
    tok_hbm,
    gate_hbm,
    value_hbm,
    down_hbm,
    gain,
    gate_scale,
    value_scale,
    gate_kernel,
    value_kernel,
    gate_bias,
    value_bias,
    osc,
    out,
    tok,
    up_all,
    down_all,
    hidden,
    stage,
    pair_in,
    peer_in,
    relay_in,
    taps,
    edge,
    edge_pre,
    par,
    wu,
    wd,
    raw_tok,
    raw_gate,
    raw_value,
    raw_down,
    sem_fetch,
    sem_own,
    sem_plane_send,
    sem_recv,
    sem_line_send,
    sem_edge,
    sem_tok_send,
    sem_tok_recv,
    sem_diag_send,
    sem_diag_recv,
    sem_tok_pair_send,
    sem_tok_pair_recv,
    sem_pair_send,
    sem_pair_recv,
    sem_peer_send,
    sem_peer_recv,
    sem_relay_send,
    sem_relay_recv,
):
    planes = depth_planes
    half = planes // 2
    me = lax.axis_index("fs")
    core = lax.axis_index("tp")
    z, p = me // GROUP, me % GROUP
    rows_own = raw_tok.shape[0]
    part_rows = rows_own // 2
    blocks, piece = wu.shape[1], wu.shape[2]
    units = hidden.shape[1]
    out_piece = wd.shape[2]
    chunk = GROUP * out_piece
    has_up, has_down = z < planes - 1, z > 0
    inner_plane = has_up & has_down
    down_kind = blocks

    def flip(mask):
        px, py = p % 2, p // 2
        return (py + mask // 2) % 2 * 2 + (px + mask % 2) % 2

    def chip(target):
        return (z * GROUP + target, core)

    others = (1, 2, 3)

    fetches = [
        pltpu.make_async_copy(src, dst, sem_fetch.at[i])
        for i, (src, dst) in enumerate(
            ((gate_hbm, raw_gate), (value_hbm, raw_value), (tok_hbm, raw_tok), (down_hbm, raw_down))
        )
    ]
    for fetch in fetches:
        fetch.start()

    barrier = pltpu.get_barrier_semaphore()
    for mask in others:
        pl.semaphore_signal(barrier, inc=1, device_id=chip(flip(mask)), device_id_type=MESH)
    pl.semaphore_signal(barrier, inc=1, device_id=(me, 1 - core), device_id_type=MESH)

    @pl.when(has_up)
    def _():
        pl.semaphore_signal(barrier, inc=1, device_id=(me + GROUP, core), device_id_type=MESH)

    @pl.when(has_down)
    def _():
        pl.semaphore_signal(barrier, inc=1, device_id=(me - GROUP, core), device_id_type=MESH)

    def remote(src, dst, send, recv, device):
        return pltpu.make_async_remote_copy(
            src_ref=src, dst_ref=dst, send_sem=send, recv_sem=recv, device_id=device, device_id_type=MESH
        )

    def up_block(j, f):
        return up_all.at[j, pl.ds(pl.multiple_of(f * piece, piece), piece), :]

    def down_block(f):
        return down_all.at[f // GROUP, :, pl.ds(pl.multiple_of(f % GROUP * out_piece, out_piece), out_piece)]

    def plane_up(j, mask):
        target = flip(mask)
        return remote(
            wu.at[target, j], up_block(j, me), sem_plane_send.at[j, mask], sem_recv.at[j, me], chip(target)
        )

    def plane_down(mask):
        target = flip(mask)
        return remote(
            wd.at[target],
            down_block(me),
            sem_plane_send.at[down_kind, mask],
            sem_recv.at[down_kind, me],
            chip(target),
        )

    def line_up(j, direction, f, src=None):
        here = up_block(j, f)
        return remote(
            here if src is None else src,
            here,
            sem_line_send.at[j, direction, f],
            sem_recv.at[j, f],
            (me + (GROUP if direction == 0 else -GROUP), core),
        )

    def line_down(direction, f, src=None):
        here = down_block(f)
        return remote(
            here if src is None else src,
            here,
            sem_line_send.at[down_kind, direction, f],
            sem_recv.at[down_kind, f],
            (me + (GROUP if direction == 0 else -GROUP), core),
        )

    def both_ways(copy_of):
        @pl.when(has_up)
        def _():
            copy_of(0).start()

        @pl.when(has_down)
        def _():
            copy_of(1).start()

    def wait_up(j, f):
        here = up_block(j, f)
        remote(here, here, sem_line_send.at[j, 0, f], sem_recv.at[j, f], (me, 1 - core)).wait_recv()

    def wait_down(f):
        here = down_block(f)
        remote(here, here, sem_line_send.at[down_kind, 0, f], sem_recv.at[down_kind, f], (me, 1 - core)).wait_recv()

    def own_up(j):
        return pltpu.make_async_copy(wu.at[p, j], up_block(j, me), sem_own.at[j])

    own_down = pltpu.make_async_copy(wd.at[p], down_block(me), sem_own.at[down_kind])

    def cast_block(j):
        for m in range(GROUP):
            first = m * units + j * 128
            wu[m, j, :, 0:128] = raw_gate[:, first : first + 128].astype(jnp.bfloat16)
            wu[m, j, :, 128:256] = raw_value[:, first : first + 128].astype(jnp.bfloat16)

    def normed(first, count):
        values = raw_tok[pl.ds(first, count), :].astype(jnp.float32)
        scaled = values * lax.rsqrt(jnp.mean(values * values, axis=1, keepdims=True) + epsilon)
        return (scaled * gain[...]).astype(jnp.bfloat16)

    fetches[0].wait()
    fetches[1].wait()
    for j in range(blocks):
        cast_block(j)
    pl.semaphore_wait(barrier, 4 + has_up.astype(jnp.int32) + has_down.astype(jnp.int32))
    for j in range(blocks):
        for mask in others:
            plane_up(j, mask).start()
        both_ways(lambda direction: line_up(j, direction, me, wu.at[p, j]))
    for j in range(blocks):
        own_up(j).start()

    def edge_slot(slot):
        return edge.at[pl.ds(pl.multiple_of(slot * EDGE, EDGE), EDGE), :]

    def edge_copy(mask):
        here = edge_slot(p + 1)
        return remote(here, here, sem_edge.at[0, mask], sem_edge.at[1, mask], chip(flip(mask)))

    edge_next = remote(
        edge_slot(GROUP), edge_slot(0), sem_edge.at[0, 0], sem_edge.at[1, 0], (me + GROUP, core)
    )

    @pl.when(jnp.logical_not(has_down))
    def _():
        edge[0:EDGE, :] = jnp.zeros_like(edge[0:EDGE, :])

    fetches[2].wait()
    edge[pl.ds(pl.multiple_of((p + 1) * EDGE, EDGE), EDGE), :] = normed(rows_own - EDGE, EDGE)
    for mask in others:
        edge_copy(mask).start()
    norm_tile = 64

    def norm_step(i, carry):
        first = pl.multiple_of(i * norm_tile, norm_tile)
        tok[pl.ds(pl.multiple_of(p * rows_own + i * norm_tile, norm_tile), norm_tile), :] = normed(first, norm_tile)
        return carry

    lax.fori_loop(0, rows_own // norm_tile, norm_step, 0)

    parts = 2
    sub_rows = part_rows // parts
    diag_rows = sub_rows // 2

    def token_rows(owner, side, part):
        start = owner * rows_own + side * part_rows + part * sub_rows
        return tok.at[pl.ds(pl.multiple_of(start, sub_rows), sub_rows), :]

    def diag_part(owner, part, which):
        start = owner * rows_own + core * part_rows + part * sub_rows + which * diag_rows
        return tok.at[pl.ds(pl.multiple_of(start, diag_rows), diag_rows), :]

    def token_copy(mask, part):
        here = token_rows(p, core, part)
        return remote(here, here, sem_tok_send.at[mask, part], sem_tok_recv.at[mask, part], chip(flip(mask)))

    def token_relay(mask, part):
        here = diag_part(flip(mask), part, mask - 1)
        return remote(
            here,
            here,
            sem_diag_send.at[mask, part],
            sem_diag_recv.at[mask, part],
            chip(flip(3 - mask)),
        )

    def token_pair(mask, part):
        here = token_rows(flip(mask), core, part)
        return remote(
            here, here, sem_tok_pair_send.at[mask, part], sem_tok_pair_recv.at[mask, part], (me, 1 - core)
        )

    for part in range(parts):
        for mask in (1, 2):
            token_copy(mask, part).start()

    fetches[3].wait()
    for m in range(GROUP):
        wd[m] = raw_down[m * units : (m + 1) * units, :].astype(jnp.bfloat16)
    own_down.start()
    for mask in others:
        plane_down(mask).start()
    for j in range(blocks):
        src = pl.ds(p * blocks + j, 1)
        cols = pl.ds(pl.multiple_of(p * units + j * 128, 128), 128)
        for side, (scale, kernel, tap_bias) in enumerate(
            ((gate_scale, gate_kernel, gate_bias), (value_scale, value_kernel, value_bias))
        ):
            dst = slice(j * 256 + side * 128, j * 256 + side * 128 + 128)
            par[0:1, dst] = scale[src, :]
            par[1:4, dst] = kernel[0:3, cols]
            par[4:5, dst] = tap_bias[src, :]

    def own_plane(j, carry):
        for mask in others:
            f = z * GROUP + flip(mask)
            wait_up(j, f)
            both_ways(lambda direction: line_up(j, direction, f))
        return carry

    lax.fori_loop(0, blocks, own_plane, 0)

    for mask in others:
        here = edge_slot(flip(mask) + 1)
        remote(here, here, sem_edge.at[0, mask], sem_edge.at[1, mask], (me, 1 - core)).wait_recv()

    @pl.when(has_up)
    def _():
        edge_next.start()

    low_half = (z < half).astype(jnp.int32)

    def plane_of(step):
        distance = (step + 1) // 2
        below = (step + low_half) % 2
        return z + distance * (1 - 2 * below), below

    def relay_one(copy_of, wait_of, below, f):
        wait_of(f)

        @pl.when((below == 1) & has_up)
        def _():
            copy_of(0, f).start()

        @pl.when((below == 0) & has_down)
        def _():
            copy_of(1, f).start()

    def relay(copy_of, wait_of, step):
        q, below = plane_of(step)

        @pl.when((q >= 0) & (q < planes))
        def _():
            def one(i, carry):
                relay_one(copy_of, wait_of, below, q * GROUP + i)
                return carry

            lax.fori_loop(0, GROUP, one, 0)

    def relay_up(j, first, last):
        def one(step, carry):
            relay(lambda direction, f: line_up(j, direction, f), lambda f: wait_up(j, f), step)
            return carry

        lax.fori_loop(first, last, one, 0)

    def wide(j):
        return pl.ds(pl.multiple_of(j * 256, 256), 256)

    def unit(owner, j):
        rows = pl.ds(pl.multiple_of(owner * rows_own, rows_own), rows_own)
        raw = jnp.dot(tok[rows, :], up_all[j], preferred_element_type=jnp.float32)
        taps[8:, :] = (raw * par[0:1, wide(j)]).astype(jnp.bfloat16).astype(jnp.float32)
        taps[0:8, :] = edge_pre[j, pl.ds(pl.multiple_of(owner * EDGE + EDGE - 8, 8), 8), :]
        conv = par[4:5, wide(j)] + par[3:4, wide(j)] * taps[8 : 8 + rows_own, :]
        conv = conv + par[2:3, wide(j)] * taps[7 : 7 + rows_own, :]
        conv = conv + par[1:2, wide(j)] * taps[6 : 6 + rows_own, :]
        g, v = conv[:, :128], conv[:, 128:]
        act = 0.5 * g * (1.0 + jnp.tanh(math.sqrt(2.0 / math.pi) * (g + 0.044715 * (g * g * g))))
        hidden[rows, pl.ds(pl.multiple_of(j * 128, 128), 128)] = (act * v).astype(jnp.bfloat16)

    def landed(mask, part):
        here = token_rows(flip(mask), core, part)
        remote(here, here, sem_tok_send.at[mask, part], sem_tok_recv.at[mask, part], (me, 1 - core)).wait_recv()

    def pair_landed(mask, part):
        there = token_rows(flip(mask), 1 - core, part)
        remote(
            there, there, sem_tok_pair_send.at[mask, part], sem_tok_pair_recv.at[mask, part], (me, 1 - core)
        ).wait_recv()

    def pass_tokens(part):
        for mask in (1, 2):
            landed(mask, part)
            token_relay(mask, part).start()
            token_pair(mask, part).start()

    def near_round(j, carry):
        relay_up(j, 1, 3)
        return carry

    lax.fori_loop(0, blocks, near_round, 0)

    part_rounds = (0, max(0, blocks - 2))

    def far_round(j, carry):
        relay_up(j, 3, 5)
        for part in range(parts):

            @pl.when(j == part_rounds[part])
            def _():
                pass_tokens(part)

        return carry

    lax.fori_loop(0, blocks, far_round, 0)

    own_down.wait()
    both_ways(lambda direction: line_down(direction, me, wd.at[p]))
    for mask in others:
        f = z * GROUP + flip(mask)
        wait_down(f)
        both_ways(lambda direction: line_down(direction, f))

    @pl.when(has_down)
    def _():
        here = edge_slot(0)
        remote(here, here, sem_edge.at[0, 0], sem_edge.at[1, 0], (me, 1 - core)).wait_recv()

    diag_round = jnp.where(inner_plane, blocks - 1, min(2, blocks - 1))

    def up_round(j, carry):
        relay_up(j, 5, 2 * planes - 1)
        own_up(j).wait()
        ahead = jnp.dot(edge[0 : GROUP * EDGE, :], up_all[j], preferred_element_type=jnp.float32)
        edge_pre[j] = (ahead * par[0:1, wide(j)]).astype(jnp.bfloat16).astype(jnp.float32)

        def group(mask, inner):
            ready = jnp.where(mask == 3, diag_round, 0)

            @pl.when((mask == 3) & (j == ready))
            def _():
                for part in range(parts):
                    for which in (0, 1):
                        here = diag_part(flip(3), part, which)
                        remote(
                            here,
                            here,
                            sem_diag_send.at[which + 1, part],
                            sem_diag_recv.at[which + 1, part],
                            (me, 1 - core),
                        ).wait_recv()
                    token_pair(3, part).start()

            @pl.when((mask > 0) & (j == ready))
            def _():
                for part in range(parts):
                    pair_landed(mask, part)

            first = jnp.where(j == ready, 0, j)
            last = jnp.where(j >= ready, j + 1, 0)

            def one(k, deeper):
                unit(flip(mask), k)
                return deeper

            return lax.fori_loop(first, last, one, inner)

        return lax.fori_loop(0, GROUP, group, carry)

    lax.fori_loop(0, blocks, up_round, 0)

    def block_rows(owner):
        return pl.ds(pl.multiple_of(owner * rows_own, rows_own), rows_own)

    strip = 2 * out_piece
    strips = chunk // strip
    per_core = half * strips

    def pair_copy(c, owner):
        return remote(
            stage.at[c, owner],
            pair_in.at[c % per_core, owner],
            sem_pair_send.at[c % per_core, owner],
            sem_pair_recv.at[c % per_core, owner],
            (me, 1 - core),
        )

    half_rows = rows_own // 2

    def half_of(which):
        return pl.ds(which * half_rows, half_rows)

    def peer_copy(c, mask, which):
        slot = (mask - 1) * 2 + which
        return remote(
            stage.at[c, flip(mask), half_of(which)],
            peer_in.at[c % per_core, mask - 1, half_of(which)],
            sem_peer_send.at[c % per_core, slot],
            sem_peer_recv.at[c % per_core, slot],
            chip(flip(mask)),
        )

    def relay_copy(c, mask):
        return remote(
            stage.at[c, flip(3), half_of(mask - 1)],
            relay_in.at[c % per_core, mask - 1],
            sem_relay_send.at[c % per_core, mask - 1],
            sem_relay_recv.at[c % per_core, mask - 1],
            chip(flip(mask)),
        )

    def combine(c, owner):
        pair_copy(c, owner).wait_recv()
        both = stage[c, owner].astype(jnp.float32) + pair_in[c % per_core, owner].astype(jnp.float32)
        stage[c, owner] = both.astype(jnp.bfloat16)

    def send_out(c):
        combine(c, flip(3))
        for mask in (1, 2):
            relay_copy(c, mask).start()
        for mask in (1, 2):
            combine(c, flip(mask))
            peer_copy(c, mask, mask - 1).start()
        combine(c, p)

    def pass_on(c):
        for mask in (1, 2):
            relay_copy(c, mask).wait_recv()
            owner = flip(3 - mask)
            rows = half_of(mask - 1)
            total = stage[c, owner, rows, :].astype(jnp.float32) + relay_in[c % per_core, mask - 1].astype(jnp.float32)
            stage[c, owner, rows, :] = total.astype(jnp.bfloat16)
            peer_copy(c, 3 - mask, mask - 1).start()

    def mine(c):
        return c // per_core == core

    def down_relay(step, carry):
        relay(line_down, wait_down, step)
        return carry

    def down_step(n, before):
        step = n // strips
        q, below = plane_of(step)
        valid = (q >= 0) & (q < planes)
        c = q * strips + n % strips
        patient = inner_plane | (step == 0)
        owed = before >= 0

        @pl.when((n == strips) & inner_plane)
        def _():
            lax.fori_loop(1, 2 * planes - 1, down_relay, 0)

        @pl.when(valid & owed & jnp.logical_not(patient))
        def _():
            pass_on(before)

        @pl.when(valid & (step > 0) & jnp.logical_not(inner_plane))
        def _():
            for i in range(GROUP // strips):
                relay_one(line_down, wait_down, below, q * GROUP + n % strips * (GROUP // strips) + i)

        @pl.when(valid)
        def _():
            cols = pl.ds(pl.multiple_of(n % strips * strip, strip), strip)

            def product(i, inner):
                owner = flip(3 - i)
                value = jnp.dot(
                    hidden[block_rows(owner), :], down_all[q, :, cols], preferred_element_type=jnp.float32
                )
                stage[c, owner] = value.astype(jnp.bfloat16)

                @pl.when(jnp.logical_not(mine(c)))
                def _():
                    pair_copy(c, owner).start()

                return inner

            lax.fori_loop(0, GROUP, product, 0)

            @pl.when(mine(c))
            def _():
                send_out(c)

        @pl.when(valid & owed & patient)
        def _():
            pass_on(before)

        return jnp.where(valid, jnp.where(mine(c), c, -1), before)

    last = lax.fori_loop(0, (2 * planes - 1) * strips, down_step, -1)

    @pl.when(last >= 0)
    def _():
        pass_on(last)

    def finish(i, carry):
        c = core * per_core + i
        total = stage[c, p].astype(jnp.float32)
        for mask in (1, 2):
            for which in (0, 1):
                peer_copy(c, mask, which).wait_recv()
            total = total + peer_in[i, mask - 1].astype(jnp.float32)
        cols = pl.ds(pl.multiple_of(i * strip, strip), strip)
        out[:, cols] = (total * osc[0:1, cols]).astype(jnp.bfloat16)
        return carry

    lax.fori_loop(0, per_core, finish, 0)

    def drain_out(i, carry):
        for mask in (1, 2):
            relay_copy(core * per_core + i, mask).wait_send()
            for which in (0, 1):
                peer_copy(core * per_core + i, mask, which).wait_send()

        def one(owner, inner):
            pair_copy((1 - core) * per_core + i, owner).wait_send()
            return inner

        return lax.fori_loop(0, GROUP, one, carry)

    lax.fori_loop(0, per_core, drain_out, 0)
    for part in range(parts):
        for mask in (1, 2):
            token_copy(mask, part).wait_send()
            token_relay(mask, part).wait_send()
        for mask in others:
            token_pair(mask, part).wait_send()
    for mask in others:
        edge_copy(mask).wait_send()
        plane_down(mask).wait_send()

    @pl.when(has_up)
    def _():
        edge_next.wait_send()

    def drain_plane(j, carry):
        for mask in others:
            plane_up(j, mask).wait_send()
        return carry

    lax.fori_loop(0, blocks, drain_plane, 0)

    def drain_line(f, carry):
        def drain_way(direction, sent):
            @pl.when(sent)
            def _():
                def one(j, inner):
                    line_up(j, direction, f).wait_send()
                    return inner

                lax.fori_loop(0, blocks, one, 0)
                line_down(direction, f).wait_send()

        drain_way(0, has_up & (f // GROUP <= z))
        drain_way(1, has_down & (f // GROUP >= z))
        return carry

    lax.fori_loop(0, planes * GROUP, drain_line, 0)


def grouped_body(count, tokens, norm_gain, gate_weight, value_weight, gate_scale, value_scale, gate_kernel, value_kernel, gate_bias, value_bias, down_weight, down_scale):
    planes = count // GROUP
    half = planes // 2
    rows, width = tokens.shape
    piece, local = gate_weight.shape
    out_piece = down_weight.shape[1]
    units = local // GROUP
    blocks = units // 128
    chunk = GROUP * out_piece
    strip = 2 * out_piece
    strips = chunk // strip
    per_core = half * strips
    dma = pltpu.SemaphoreType.DMA
    bf16, f32 = jnp.bfloat16, jnp.float32
    vmem = pl.BlockSpec(memory_space=pltpu.VMEM)
    hbm = pl.BlockSpec(memory_space=pl.ANY)
    return pl.pallas_call(
        functools.partial(fused_kernel, planes),
        out_shape=jax.ShapeDtypeStruct((rows, half * chunk), bf16),
        in_specs=[hbm] * 4 + [vmem] * 8,
        out_specs=vmem,
        scratch_shapes=[
            pltpu.VMEM((GROUP * rows, width), bf16),
            pltpu.VMEM((blocks, width, 256), bf16),
            pltpu.VMEM((planes, units, chunk), bf16),
            pltpu.VMEM((GROUP * rows, units), bf16),
            pltpu.VMEM((2 * per_core, GROUP, rows, strip), bf16),
            pltpu.VMEM((per_core, GROUP, rows, strip), bf16),
            pltpu.VMEM((per_core, 2, rows, strip), bf16),
            pltpu.VMEM((per_core, 2, rows // 2, strip), bf16),
            pltpu.VMEM((rows + 8, 256), f32),
            pltpu.VMEM(((GROUP + 1) * EDGE, width), bf16),
            pltpu.VMEM((blocks, GROUP * EDGE, 256), f32),
            pltpu.VMEM((8, 2 * units), f32),
            pltpu.VMEM((GROUP, blocks, piece, 256), bf16),
            pltpu.VMEM((GROUP, units, out_piece), bf16),
            pltpu.VMEM((rows, width), bf16),
            pltpu.VMEM((piece, local), f32),
            pltpu.VMEM((piece, local), f32),
            pltpu.VMEM((local, out_piece), f32),
            dma((4,)),
            dma((blocks + 1,)),
            dma((blocks + 1, GROUP)),
            dma((blocks + 1, count)),
            dma((blocks + 1, 2, count)),
            dma((2, GROUP)),
            dma((GROUP, 2)),
            dma((GROUP, 2)),
            dma((GROUP, 2)),
            dma((GROUP, 2)),
            dma((GROUP, 2)),
            dma((GROUP, 2)),
            dma((per_core, GROUP)),
            dma((per_core, GROUP)),
            dma((per_core, 4)),
            dma((per_core, 4)),
            dma((per_core, 2)),
            dma((per_core, 2)),
        ],
        compiler_params=pltpu.CompilerParams(
            collective_id=0, has_side_effects=True, vmem_limit_bytes=67043328
        ),
    )(
        tokens,
        gate_weight,
        value_weight,
        down_weight,
        norm_gain[None, :],
        gate_scale.reshape(-1, 128),
        value_scale.reshape(-1, 128),
        gate_kernel,
        value_kernel,
        gate_bias.reshape(-1, 128),
        value_bias.reshape(-1, 128),
        down_scale[None, :],
    )


def solution(mesh):
    count, tp = mesh.shape["fs"], mesh.shape["tp"]

    def whole(*arrays):
        local = arrays[2].shape[1]
        fits = tp == 2 and count % (2 * GROUP) == 0 and local % (GROUP * 128) == 0
        if fits:
            return grouped_body(count, *arrays)
        return body(*arrays)

    return jax.shard_map(
        whole,
        mesh=mesh,
        in_specs=(
            P("fs", None),
            P(),
            P("fs", "tp"),
            P("fs", "tp"),
            P("tp"),
            P("tp"),
            P(None, "tp"),
            P(None, "tp"),
            P("tp"),
            P("tp"),
            P("tp", "fs"),
            P("tp"),
        ),
        out_specs=P("fs", "tp"),
        check_vma=False,
    )
```

time: 218 us -> 170 us (0.78)
  Pallas kernels: 210 us -> 166 us
  local copies, waits for them, and re-layouts: 7.91 us -> 2.67 us
    pallas_call x1, Pallas kernels: 210 us -> 166 us  [grouped_body(): pl.pallas_call(functools.partial(fused_kernel, planes), out_shape=jax.Sha...]
    broadcast_in_dim x4 -> x0, local copies, waits for them, and re-layouts: 5.24 us -> none  [the longest x1 1.31 us: grouped_body(): gate_scale[None, :]]
where the time goes in v1:
time: 170 us; the launch traced here: 169 us
  Pallas kernels  166 us (98%)
  local copies, waits for them, and re-layouts  2.67 us (2%)
    pallas_call x1, Pallas kernels, grouped_body(): pl.pallas_call(functools.partial(fused_kernel, planes), out_shape=jax.Sha...  166 us

profile of v1, /device:TPU:1, one launch (start us, length us, event | category | flops | bytes accessed | tf_op | source)
XLA Modules:
  0.0 168.7 jit_solution(8526639400894308052)
XLA Ops:
  0.0 166.1 %shard_map.118 = bf16[768,1024]{1,0:T(8,128)(2,1)} custom-call(bf16[768,2048]{1,0:T(8,128)(2,1)} %tok_hbm.1, f32[128,2560]{1,0:T(8,128)} %gate_hbm.1, f32[128,2560]{1,0:T(8,128)} %value_hbm.1, f32[2560,128]{1,0:T(8,128)} %down_hbm.1, f32[1,2048]{1,0:T(1,128)} %bitcast.10, f32[20,128]{1,0:T(8,128)} %bitcast.6, f32[20,128]{1,0:T(8,128)} %bitcast.7, ...), custom_call_target="tpu_custom_call" | custom-call | tf_op jit(solution)/shard_map/pallas_call | solution.py:721
  166.1 2.7 %copy.14 = bf16[768,1024]{1,0:T(8,128)(2,1)} copy(bf16[768,1024]{1,0:T(8,128)(2,1)} %shard_map.118) | data formatting | bytes 3145728

commit v2 on v1

--- a/solution.py
+++ b/solution.py
@@ -117,8 +117,15 @@
     sem_fetch,
     sem_own,
     sem_plane_send,
-    sem_recv,
-    sem_line_send,
+    sem_plane_recv,
+    sem_first_send,
+    sem_first_recv,
+    sem_piece_send,
+    sem_piece_recv,
+    sem_far_send,
+    sem_far_recv,
+    sem_down_send,
+    sem_down_recv,
     sem_edge,
     sem_tok_send,
     sem_tok_recv,
@@ -146,7 +153,9 @@
     chunk = GROUP * out_piece
     has_up, has_down = z < planes - 1, z > 0
     inner_plane = has_up & has_down
-    down_kind = blocks
+    end_plane = jnp.logical_not(inner_plane)
+    cut = min(2, blocks - 1)
+    groups = ((0, cut), (cut, blocks))
 
     def flip(mask):
         px, py = p % 2, p // 2
@@ -184,47 +193,84 @@
             src_ref=src, dst_ref=dst, send_sem=send, recv_sem=recv, device_id=device, device_id_type=MESH
         )
 
-    def up_block(j, f):
-        return up_all.at[j, pl.ds(pl.multiple_of(f * piece, piece), piece), :]
+    def rows_of(f, count=1):
+        return pl.ds(pl.multiple_of(f * piece, piece), count * piece)
 
     def down_block(f):
         return down_all.at[f // GROUP, :, pl.ds(pl.multiple_of(f % GROUP * out_piece, out_piece), out_piece)]
 
-    def plane_up(j, mask):
-        target = flip(mask)
+    def line(side):
+        return (me + (GROUP if side == 0 else -GROUP), core)
+
+    def plane_up(g, mask):
+        first, last = groups[g]
         return remote(
-            wu.at[target, j], up_block(j, me), sem_plane_send.at[j, mask], sem_recv.at[j, me], chip(target)
-        )
+            wu.at[flip(mask), first:last],
+            up_all.at[first:last, rows_of(me), :],
+            sem_plane_send.at[g, mask],
+            sem_plane_recv.at[g, mask],
+            chip(flip(mask)),
+        )
+
+    def plane_up_landed(g, mask):
+        first, last = groups[g]
+        here = up_all.at[first:last, rows_of(z * GROUP + flip(mask)), :]
+        remote(here, here, sem_plane_send.at[g, mask], sem_plane_recv.at[g, mask], chip(flip(mask))).wait_recv()
+
+    def first_hop(side, g, mask):
+        first, last = groups[g]
+        there = up_all.at[first:last, rows_of(z * GROUP + flip(mask)), :]
+        here = there if mask else wu.at[p, first:last]
+        return remote(here, there, sem_first_send.at[side, g, mask], sem_first_recv.at[side, g, mask], line(side))
+
+    def first_landed(side, g, mask):
+        first, last = groups[g]
+        q = z + (2 * side - 1)
+        here = up_all.at[first:last, rows_of(q * GROUP + flip(mask)), :]
+        remote(
+            here, here, sem_first_send.at[side, g, mask], sem_first_recv.at[side, g, mask], (me, 1 - core)
+        ).wait_recv()
+
+    def piece_hop(side, mask):
+        here = up_all.at[:, rows_of((z + (2 * side - 1)) * GROUP + flip(mask)), :]
+        return remote(here, here, sem_piece_send.at[mask], sem_piece_recv.at[mask], line(side))
+
+    def piece_landed(side, mask):
+        here = up_all.at[:, rows_of((z + 2 * (2 * side - 1)) * GROUP + flip(mask)), :]
+        remote(here, here, sem_piece_send.at[mask], sem_piece_recv.at[mask], (me, 1 - core)).wait_recv()
+
+    def far_hop(side, distance, j):
+        q = z + distance * (2 * side - 1)
+        here = up_all.at[j, rows_of(q * GROUP, GROUP), :]
+        return remote(
+            here, here, sem_far_send.at[side, distance - 1, j], sem_far_recv.at[side, distance - 1, j], line(side)
+        )
+
+    def far_landed(side, distance, j):
+        q = z + distance * (2 * side - 1)
+        here = up_all.at[j, rows_of(q * GROUP, GROUP), :]
+        remote(
+            here, here, sem_far_send.at[side, distance - 2, j], sem_far_recv.at[side, distance - 2, j], (me, 1 - core)
+        ).wait_recv()
 
     def plane_down(mask):
-        target = flip(mask)
         return remote(
-            wd.at[target],
+            wd.at[flip(mask)],
             down_block(me),
-            sem_plane_send.at[down_kind, mask],
-            sem_recv.at[down_kind, me],
-            chip(target),
-        )
-
-    def line_up(j, direction, f, src=None):
-        here = up_block(j, f)
-        return remote(
-            here if src is None else src,
-            here,
-            sem_line_send.at[j, direction, f],
-            sem_recv.at[j, f],
-            (me + (GROUP if direction == 0 else -GROUP), core),
-        )
-
-    def line_down(direction, f, src=None):
+            sem_plane_send.at[2, mask],
+            sem_down_recv.at[me],
+            chip(flip(mask)),
+        )
+
+    def line_down(side, f, slot, src=None):
         here = down_block(f)
         return remote(
-            here if src is None else src,
-            here,
-            sem_line_send.at[down_kind, direction, f],
-            sem_recv.at[down_kind, f],
-            (me + (GROUP if direction == 0 else -GROUP), core),
-        )
+            here if src is None else src, here, sem_down_send.at[slot], sem_down_recv.at[f], line(side)
+        )
+
+    def wait_down(f):
+        here = down_block(f)
+        remote(here, here, sem_down_send.at[f], sem_down_recv.at[f], (me, 1 - core)).wait_recv()
 
     def both_ways(copy_of):
         @pl.when(has_up)
@@ -235,18 +281,8 @@
         def _():
             copy_of(1).start()
 
-    def wait_up(j, f):
-        here = up_block(j, f)
-        remote(here, here, sem_line_send.at[j, 0, f], sem_recv.at[j, f], (me, 1 - core)).wait_recv()
-
-    def wait_down(f):
-        here = down_block(f)
-        remote(here, here, sem_line_send.at[down_kind, 0, f], sem_recv.at[down_kind, f], (me, 1 - core)).wait_recv()
-
-    def own_up(j):
-        return pltpu.make_async_copy(wu.at[p, j], up_block(j, me), sem_own.at[j])
-
-    own_down = pltpu.make_async_copy(wd.at[p], down_block(me), sem_own.at[down_kind])
+    own_up = pltpu.make_async_copy(wu.at[p], up_all.at[:, rows_of(me), :], sem_own.at[0])
+    own_down = pltpu.make_async_copy(wd.at[p], down_block(me), sem_own.at[1])
 
     def cast_block(j):
         for m in range(GROUP):
@@ -264,12 +300,11 @@
     for j in range(blocks):
         cast_block(j)
     pl.semaphore_wait(barrier, 4 + has_up.astype(jnp.int32) + has_down.astype(jnp.int32))
-    for j in range(blocks):
+    for g in range(2):
         for mask in others:
-            plane_up(j, mask).start()
-        both_ways(lambda direction: line_up(j, direction, me, wu.at[p, j]))
-    for j in range(blocks):
-        own_up(j).start()
+            plane_up(g, mask).start()
+        both_ways(lambda side: first_hop(side, g, 0))
+    own_up.start()
 
     def edge_slot(slot):
         return edge.at[pl.ds(pl.multiple_of(slot * EDGE, EDGE), EDGE), :]
@@ -313,22 +348,22 @@
 
     def token_copy(mask, part):
         here = token_rows(p, core, part)
-        return remote(here, here, sem_tok_send.at[mask, part], sem_tok_recv.at[mask, part], chip(flip(mask)))
+        return remote(here, here, sem_tok_send.at[mask - 1, part], sem_tok_recv.at[mask - 1, part], chip(flip(mask)))
 
     def token_relay(mask, part):
         here = diag_part(flip(mask), part, mask - 1)
         return remote(
             here,
             here,
-            sem_diag_send.at[mask, part],
-            sem_diag_recv.at[mask, part],
+            sem_diag_send.at[mask - 1, part],
+            sem_diag_recv.at[mask - 1, part],
             chip(flip(3 - mask)),
         )
 
     def token_pair(mask, part):
         here = token_rows(flip(mask), core, part)
         return remote(
-            here, here, sem_tok_pair_send.at[mask, part], sem_tok_pair_recv.at[mask, part], (me, 1 - core)
+            here, here, sem_tok_pair_send.at[mask - 1, part], sem_tok_pair_recv.at[mask - 1, part], (me, 1 - core)
         )
 
     for part in range(parts):
@@ -339,8 +374,6 @@
     for m in range(GROUP):
         wd[m] = raw_down[m * units : (m + 1) * units, :].astype(jnp.bfloat16)
     own_down.start()
-    for mask in others:
-        plane_down(mask).start()
     for j in range(blocks):
         src = pl.ds(p * blocks + j, 1)
         cols = pl.ds(pl.multiple_of(p * units + j * 128, 128), 128)
@@ -348,18 +381,13 @@
             ((gate_scale, gate_kernel, gate_bias), (value_scale, value_kernel, value_bias))
         ):
             dst = slice(j * 256 + side * 128, j * 256 + side * 128 + 128)
-            par[0:1, dst] = scale[src, :]
-            par[1:4, dst] = kernel[0:3, cols]
+            par[1:4, dst] = kernel[0:3, cols] * scale[src, :]
             par[4:5, dst] = tap_bias[src, :]
 
-    def own_plane(j, carry):
+    for g in range(2):
         for mask in others:
-            f = z * GROUP + flip(mask)
-            wait_up(j, f)
-            both_ways(lambda direction: line_up(j, direction, f))
-        return carry
-
-    lax.fori_loop(0, blocks, own_plane, 0)
+            plane_up_landed(g, mask)
+            both_ways(lambda side: first_hop(side, g, mask))
 
     for mask in others:
         here = edge_slot(flip(mask) + 1)
@@ -376,58 +404,29 @@
         below = (step + low_half) % 2
         return z + distance * (1 - 2 * below), below
 
-    def relay_one(copy_of, wait_of, below, f):
-        wait_of(f)
-
-        @pl.when((below == 1) & has_up)
-        def _():
-            copy_of(0, f).start()
-
-        @pl.when((below == 0) & has_down)
-        def _():
-            copy_of(1, f).start()
-
-    def relay(copy_of, wait_of, step):
-        q, below = plane_of(step)
-
-        @pl.when((q >= 0) & (q < planes))
-        def _():
-            def one(i, carry):
-                relay_one(copy_of, wait_of, below, q * GROUP + i)
-                return carry
-
-            lax.fori_loop(0, GROUP, one, 0)
-
-    def relay_up(j, first, last):
-        def one(step, carry):
-            relay(lambda direction, f: line_up(j, direction, f), lambda f: wait_up(j, f), step)
-            return carry
-
-        lax.fori_loop(first, last, one, 0)
-
     def wide(j):
         return pl.ds(pl.multiple_of(j * 256, 256), 256)
 
     def unit(owner, j):
         rows = pl.ds(pl.multiple_of(owner * rows_own, rows_own), rows_own)
-        raw = jnp.dot(tok[rows, :], up_all[j], preferred_element_type=jnp.float32)
-        taps[8:, :] = (raw * par[0:1, wide(j)]).astype(jnp.bfloat16).astype(jnp.float32)
+        taps[8:, :] = jnp.dot(tok[rows, :], up_all[j], preferred_element_type=jnp.float32)
         taps[0:8, :] = edge_pre[j, pl.ds(pl.multiple_of(owner * EDGE + EDGE - 8, 8), 8), :]
         conv = par[4:5, wide(j)] + par[3:4, wide(j)] * taps[8 : 8 + rows_own, :]
         conv = conv + par[2:3, wide(j)] * taps[7 : 7 + rows_own, :]
         conv = conv + par[1:2, wide(j)] * taps[6 : 6 + rows_own, :]
         g, v = conv[:, :128], conv[:, 128:]
-        act = 0.5 * g * (1.0 + jnp.tanh(math.sqrt(2.0 / math.pi) * (g + 0.044715 * (g * g * g))))
-        hidden[rows, pl.ds(pl.multiple_of(j * 128, 128), 128)] = (act * v).astype(jnp.bfloat16)
+        root = math.sqrt(2.0 / math.pi)
+        bend = jnp.tanh(g * (root + (root * 0.044715) * (g * g)))
+        hidden[rows, pl.ds(pl.multiple_of(j * 128, 128), 128)] = ((0.5 * (g * v)) * (1.0 + bend)).astype(jnp.bfloat16)
 
     def landed(mask, part):
         here = token_rows(flip(mask), core, part)
-        remote(here, here, sem_tok_send.at[mask, part], sem_tok_recv.at[mask, part], (me, 1 - core)).wait_recv()
+        remote(here, here, sem_tok_send.at[mask - 1, part], sem_tok_recv.at[mask - 1, part], (me, 1 - core)).wait_recv()
 
     def pair_landed(mask, part):
         there = token_rows(flip(mask), 1 - core, part)
         remote(
-            there, there, sem_tok_pair_send.at[mask, part], sem_tok_pair_recv.at[mask, part], (me, 1 - core)
+            there, there, sem_tok_pair_send.at[mask - 1, part], sem_tok_pair_recv.at[mask - 1, part], (me, 1 - core)
         ).wait_recv()
 
     def pass_tokens(part):
@@ -436,80 +435,101 @@
             token_relay(mask, part).start()
             token_pair(mask, part).start()
 
-    def near_round(j, carry):
-        relay_up(j, 1, 3)
-        return carry
-
-    lax.fori_loop(0, blocks, near_round, 0)
-
-    part_rounds = (0, max(0, blocks - 2))
-
-    def far_round(j, carry):
-        relay_up(j, 3, 5)
-        for part in range(parts):
-
-            @pl.when(j == part_rounds[part])
-            def _():
-                pass_tokens(part)
-
-        return carry
-
-    lax.fori_loop(0, blocks, far_round, 0)
-
-    own_down.wait()
-    both_ways(lambda direction: line_down(direction, me, wd.at[p]))
-    for mask in others:
-        f = z * GROUP + flip(mask)
-        wait_down(f)
-        both_ways(lambda direction: line_down(direction, f))
+    def near(side):
+        def pieces():
+            for mask in range(GROUP):
+                for g in range(2):
+                    first_landed(side, g, mask)
+                piece_hop(side, mask).start()
+
+        def whole():
+            for mask in range(GROUP):
+                for g in range(2):
+                    first_landed(side, g, mask)
+
+        onward = z + (1 - 2 * side)
+        into_end = onward == (planes - 1 if side == 0 else 0)
+
+        @pl.when(inner_plane & into_end)
+        def _():
+            pieces()
+
+        @pl.when(inner_plane & jnp.logical_not(into_end))
+        def _():
+            whole()
+
+            def one(j, carry):
+                far_hop(side, 1, j).start()
+                return carry
+
+            lax.fori_loop(0, blocks, one, 0)
+
+        @pl.when(end_plane & (has_down if side == 0 else has_up))
+        def _():
+            whole()
+
+    @pl.when(low_half == 1)
+    def _():
+        near(1)
+        near(0)
+
+    @pl.when(low_half == 0)
+    def _():
+        near(0)
+        near(1)
+
+    pass_tokens(0)
+
+    def send_down():
+        for mask in others:
+            plane_down(mask).start()
+
+    def pass_rest():
+        pass_tokens(parts - 1)
+        send_down()
+
+    @pl.when(end_plane)
+    def _():
+        for mask in range(GROUP):
+            for side in (0, 1):
+
+                @pl.when((z >= 2) if side == 0 else (z < planes - 2))
+                def _():
+                    piece_landed(side, mask)
+
+            if mask == GROUP - 2:
+                pass_rest()
 
     @pl.when(has_down)
     def _():
         here = edge_slot(0)
         remote(here, here, sem_edge.at[0, 0], sem_edge.at[1, 0], (me, 1 - core)).wait_recv()
 
-    diag_round = jnp.where(inner_plane, blocks - 1, min(2, blocks - 1))
-
-    def up_round(j, carry):
-        relay_up(j, 5, 2 * planes - 1)
-        own_up(j).wait()
+    own_up.wait()
+    own_down.wait()
+
+    def edge_block(j):
         ahead = jnp.dot(edge[0 : GROUP * EDGE, :], up_all[j], preferred_element_type=jnp.float32)
-        edge_pre[j] = (ahead * par[0:1, wide(j)]).astype(jnp.bfloat16).astype(jnp.float32)
-
-        def group(mask, inner):
-            ready = jnp.where(mask == 3, diag_round, 0)
-
-            @pl.when((mask == 3) & (j == ready))
+        edge_pre[j] = ahead
+
+    def far_round(j, carry):
+        @pl.when(inner_plane)
+        def _():
+            for distance in range(2, planes - 1):
+                for side in (0, 1):
+
+                    @pl.when((z >= distance) if side == 0 else (z < planes - distance))
+                    def _():
+                        far_landed(side, distance, j)
+                        far_hop(side, distance, j).start()
+
+            @pl.when(j == max(0, blocks - 2))
             def _():
-                for part in range(parts):
-                    for which in (0, 1):
-                        here = diag_part(flip(3), part, which)
-                        remote(
-                            here,
-                            here,
-                            sem_diag_send.at[which + 1, part],
-                            sem_diag_recv.at[which + 1, part],
-                            (me, 1 - core),
-                        ).wait_recv()
-                    token_pair(3, part).start()
-
-            @pl.when((mask > 0) & (j == ready))
-            def _():
-                for part in range(parts):
-                    pair_landed(mask, part)
-
-            first = jnp.where(j == ready, 0, j)
-            last = jnp.where(j >= ready, j + 1, 0)
-
-            def one(k, deeper):
-                unit(flip(mask), k)
-                return deeper
-
-            return lax.fori_loop(first, last, one, inner)
-
-        return lax.fori_loop(0, GROUP, group, carry)
-
-    lax.fori_loop(0, blocks, up_round, 0)
+                pass_rest()
+
+        return carry
+
+    lax.fori_loop(0, blocks, far_round, 0)
 
     def block_rows(owner):
         return pl.ds(pl.multiple_of(owner * rows_own, rows_own), rows_own)
@@ -530,7 +550,7 @@
     half_rows = rows_own // 2
 
     def half_of(which):
-        return pl.ds(which * half_rows, half_rows)
+        return pl.ds(pl.multiple_of(which * half_rows, half_rows), half_rows)
 
     def peer_copy(c, mask, which):
         slot = (mask - 1) * 2 + which
@@ -556,14 +576,28 @@
         both = stage[c, owner].astype(jnp.float32) + pair_in[c % per_core, owner].astype(jnp.float32)
         stage[c, owner] = both.astype(jnp.bfloat16)
 
-    def send_out(c):
-        combine(c, flip(3))
-        for mask in (1, 2):
-            relay_copy(c, mask).start()
-        for mask in (1, 2):
-            combine(c, flip(mask))
+    def product(c, owner):
+        first = pl.multiple_of(c % strips * strip, strip)
+        value = jnp.dot(
+            hidden[block_rows(owner), :], down_all[c // strips, :, pl.ds(first, strip)], preferred_element_type=jnp.float32
+        )
+        stage[c, owner] = value.astype(jnp.bfloat16)
+
+        @pl.when(jnp.logical_not(mine(c)))
+        def _():
+            pair_copy(c, owner).start()
+
+    def send_out(c, mask):
+        combine(c, flip(mask))
+
+        @pl.when(mask == 3)
+        def _():
+            for way in (1, 2):
+                relay_copy(c, way).start()
+
+        @pl.when((mask == 1) | (mask == 2))
+        def _():
             peer_copy(c, mask, mask - 1).start()
-        combine(c, p)
 
     def pass_on(c):
         for mask in (1, 2):
@@ -577,68 +611,210 @@
     def mine(c):
         return c // per_core == core
 
-    def down_relay(step, carry):
-        relay(line_down, wait_down, step)
-        return carry
+    def own_down_out():
+        both_ways(lambda side: line_down(side, me, me if side == 0 else planes * GROUP + p, wd.at[p]))
+        for mask in others:
+            f = z * GROUP + flip(mask)
+            wait_down(f)
+            both_ways(lambda side: line_down(side, f, f if side == 0 else planes * GROUP + flip(mask)))
+
+    diag_round = jnp.where(inner_plane, blocks - 1, min(2, blocks - 1))
+
+    def up_round(j, carry):
+        @pl.when(end_plane)
+        def _():
+            for distance in range(3, planes):
+                for side in (0, 1):
+
+                    @pl.when((z >= distance) if side == 0 else (z < planes - distance))
+                    def _():
+                        far_landed(side, distance, j)
+
+        edge_block(j)
+
+        @pl.when(j == diag_round)
+        def _():
+            for part in range(parts):
+                for which in (0, 1):
+                    here = diag_part(flip(3), part, which)
+                    remote(
+                        here,
+                        here,
+                        sem_diag_send.at[which, part],
+                        sem_diag_recv.at[which, part],
+                        (me, 1 - core),
+                    ).wait_recv()
+                token_pair(3, part).start()
+
+        final = j == blocks - 1
+
+        def group(i, inner):
+            mask = jnp.where(final, 3 - i, i)
+            ready = jnp.where(mask == 3, diag_round, 0)
+
+            @pl.when((mask == 3) & (j == diag_round))
+            def _():
+                own_down_out()
+
+            @pl.when((mask > 0) & (j == ready))
+            def _():
+                for part in range(parts):
+                    pair_landed(mask, part)
+
+            first = jnp.where(j == ready, 0, j)
+            last = jnp.where(j >= ready, j + 1, 0)
+
+            def one(k, deeper):
+                unit(flip(mask), k)
+                return deeper
+
+            lax.fori_loop(first, last, one, inner)
+
+            @pl.when(final)
+            def _():
+                for n in range(strips):
+                    product(z * strips + n, flip(mask))
+
+                @pl.when(mine(z * strips) & (i > 0))
+                def _():
+                    for n in range(strips):
+                        send_out(z * strips + n, mask + 1)
+
+            return inner
+
+        return lax.fori_loop(0, GROUP, group, carry)
+
+    lax.fori_loop(0, blocks, up_round, 0)
+
+    @pl.when(mine(z * strips))
+    def _():
+        for n in range(strips):
+            send_out(z * strips + n, 0)
+        for n in range(strips - 1):
+            pass_on(z * strips + n)
+
+    def pass_plane(step):
+        q, below = plane_of(step)
+
+        @pl.when((q >= 0) & (q < planes))
+        def _():
+            def one(i, carry):
+                f = q * GROUP + i
+                wait_down(f)
+
+                @pl.when((below == 1) & has_up)
+                def _():
+                    line_down(0, f, f).start()
+
+                @pl.when((below == 0) & has_down)
+                def _():
+                    line_down(1, f, f).start()
+
+                return carry
+
+            lax.fori_loop(0, GROUP, one, 0)
+
+    def drain_early():
+        for part in range(parts):
+            for mask in (1, 2):
+                token_copy(mask, part).wait_send()
+                token_relay(mask, part).wait_send()
+            for mask in others:
+                token_pair(mask, part).wait_send()
+        for mask in others:
+            edge_copy(mask).wait_send()
+            plane_down(mask).wait_send()
+            for g in range(2):
+                plane_up(g, mask).wait_send()
+
+        @pl.when(has_up)
+        def _():
+            edge_next.wait_send()
+
+        for side in (0, 1):
+
+            @pl.when(has_up if side == 0 else has_down)
+            def _():
+                for g in range(2):
+                    for mask in range(GROUP):
+                        first_hop(side, g, mask).wait_send()
+
+            onward = z + (1 - 2 * side)
+            into_end = onward == (planes - 1 if side == 0 else 0)
+
+            @pl.when(inner_plane & into_end)
+            def _():
+                for mask in range(GROUP):
+                    piece_hop(side, mask).wait_send()
+
+            @pl.when(inner_plane)
+            def _():
+                for distance in range(1, planes - 1):
+                    valid = (z >= distance) if side == 0 else (z < planes - distance)
+
+                    @pl.when(valid & (jnp.logical_not(into_end) if distance == 1 else True))
+                    def _():
+                        def one(j, carry):
+                            far_hop(side, distance, j).wait_send()
+                            return carry
+
+                        lax.fori_loop(0, blocks, one, 0)
 
     def down_step(n, before):
         step = n // strips
         q, below = plane_of(step)
         valid = (q >= 0) & (q < planes)
         c = q * strips + n % strips
-        patient = inner_plane | (step == 0)
         owed = before >= 0
 
         @pl.when((n == strips) & inner_plane)
         def _():
-            lax.fori_loop(1, 2 * planes - 1, down_relay, 0)
-
-        @pl.when(valid & owed & jnp.logical_not(patient))
-        def _():
-            pass_on(before)
-
-        @pl.when(valid & (step > 0) & jnp.logical_not(inner_plane))
+            pass_plane(1)
+            pass_plane(2)
+
+        @pl.when(n == 2 * strips)
+        def _():
+            drain_early()
+
+        @pl.when((n == 2 * strips + 1) & inner_plane)
+        def _():
+            for later in range(3, 2 * planes - 1):
+                pass_plane(later)
+
+        @pl.when(valid & end_plane)
         def _():
             for i in range(GROUP // strips):
-                relay_one(line_down, wait_down, below, q * GROUP + n % strips * (GROUP // strips) + i)
+                wait_down(q * GROUP + n % strips * (GROUP // strips) + i)
 
         @pl.when(valid)
         def _():
-            cols = pl.ds(pl.multiple_of(n % strips * strip, strip), strip)
-
-            def product(i, inner):
-                owner = flip(3 - i)
-                value = jnp.dot(
-                    hidden[block_rows(owner), :], down_all[q, :, cols], preferred_element_type=jnp.float32
-                )
-                stage[c, owner] = value.astype(jnp.bfloat16)
-
-                @pl.when(jnp.logical_not(mine(c)))
-                def _():
-                    pair_copy(c, owner).start()
-
+            def one(i, inner):
+                product(c, flip(3 - i))
                 return inner
 
-            lax.fori_loop(0, GROUP, product, 0)
+            lax.fori_loop(0, GROUP, one, 0)
 
             @pl.when(mine(c))
             def _():
-                send_out(c)
-
-        @pl.when(valid & owed & patient)
+                def one(i, inner):
+                    send_out(c, 3 - i)
+                    return inner
+
+                lax.fori_loop(0, GROUP, one, 0)
+
+        due = valid & owed & (mine(c) | (n % strips == strips - 1))
+
+        @pl.when(due)
         def _():
             pass_on(before)
 
-        return jnp.where(valid, jnp.where(mine(c), c, -1), before)
-
-    last = lax.fori_loop(0, (2 * planes - 1) * strips, down_step, -1)
-
-    @pl.when(last >= 0)
-    def _():
-        pass_on(last)
-
-    def finish(i, carry):
-        c = core * per_core + i
+        return jnp.where(valid & mine(c), c, jnp.where(due, -1, before))
+
+    first_owed = jnp.where(mine(z * strips), z * strips + strips - 1, -1)
+    last = lax.fori_loop(strips, (2 * planes - 1) * strips, down_step, first_owed)
+
+    def finish(c):
+        i = c % per_core
         total = stage[c, p].astype(jnp.float32)
         for mask in (1, 2):
             for which in (0, 1):
@@ -646,9 +822,16 @@
             total = total + peer_in[i, mask - 1].astype(jnp.float32)
         cols = pl.ds(pl.multiple_of(i * strip, strip), strip)
         out[:, cols] = (total * osc[0:1, cols]).astype(jnp.bfloat16)
+
+    @pl.when(last >= 0)
+    def _():
+        pass_on(last)
+
+    def finish_one(i, carry):
+        finish(core * per_core + i)
         return carry
 
-    lax.fori_loop(0, per_core, finish, 0)
+    lax.fori_loop(0, per_core, finish_one, 0)
 
     def drain_out(i, carry):
         for mask in (1, 2):
@@ -663,43 +846,29 @@
         return lax.fori_loop(0, GROUP, one, carry)
 
     lax.fori_loop(0, per_core, drain_out, 0)
-    for part in range(parts):
-        for mask in (1, 2):
-            token_copy(mask, part).wait_send()
-            token_relay(mask, part).wait_send()
-        for mask in others:
-            token_pair(mask, part).wait_send()
-    for mask in others:
-        edge_copy(mask).wait_send()
-        plane_down(mask).wait_send()
-
-    @pl.when(has_up)
-    def _():
-        edge_next.wait_send()
-
-    def drain_plane(j, carry):
-        for mask in others:
-            plane_up(j, mask).wait_send()
-        return carry
-
-    lax.fori_loop(0, blocks, drain_plane, 0)
-
-    def drain_line(f, carry):
-        def drain_way(direction, sent):
-            @pl.when(sent)
+
+    for side in (0, 1):
+
+        @pl.when(has_up if side == 0 else has_down)
+        def _():
+            for mask in range(GROUP):
+                f = z * GROUP + flip(mask)
+                line_down(side, f, f if side == 0 else planes * GROUP + flip(mask)).wait_send()
+
+    @pl.when(inner_plane)
+    def _():
+        def drain_down(f, carry):
+            @pl.when(f // GROUP < z)
             def _():
-                def one(j, inner):
-                    line_up(j, direction, f).wait_send()
-                    return inner
-
-                lax.fori_loop(0, blocks, one, 0)
-                line_down(direction, f).wait_send()
-
-        drain_way(0, has_up & (f // GROUP <= z))
-        drain_way(1, has_down & (f // GROUP >= z))
-        return carry
-
-    lax.fori_loop(0, planes * GROUP, drain_line, 0)
+                line_down(0, f, f).wait_send()
+
+            @pl.when(f // GROUP > z)
+            def _():
+                line_down(1, f, f).wait_send()
+
+            return carry
+
+        lax.fori_loop(0, planes * GROUP, drain_down, 0)
 
 
 def grouped_body(count, tokens, norm_gain, gate_weight, value_weight, gate_scale, value_scale, gate_kernel, value_kernel, gate_bias, value_bias, down_weight, down_scale):
@@ -743,17 +912,24 @@
             pltpu.VMEM((piece, local), f32),
             pltpu.VMEM((local, out_piece), f32),
             dma((4,)),
-            dma((blocks + 1,)),
-            dma((blocks + 1, GROUP)),
-            dma((blocks + 1, count)),
-            dma((blocks + 1, 2, count)),
+            dma((2,)),
+            dma((3, GROUP)),
             dma((2, GROUP)),
-            dma((GROUP, 2)),
-            dma((GROUP, 2)),
-            dma((GROUP, 2)),
-            dma((GROUP, 2)),
-            dma((GROUP, 2)),
-            dma((GROUP, 2)),
+            dma((2, 2, GROUP)),
+            dma((2, 2, GROUP)),
+            dma((GROUP,)),
+            dma((GROUP,)),
+            dma((2, max(1, planes - 2), blocks)),
+            dma((2, max(1, planes - 2), blocks)),
+            dma((count + GROUP,)),
+            dma((count,)),
+            dma((2, GROUP)),
+            dma((2, 2)),
+            dma((2, 2)),
+            dma((2, 2)),
+            dma((2, 2)),
+            dma((3, 2)),
+            dma((3, 2)),
             dma((per_core, GROUP)),
             dma((per_core, GROUP)),
             dma((per_core, 4)),

time: 170 us -> 161 us (0.947)
  Pallas kernels: 166 us -> 158 us
    pallas_call x1, Pallas kernels: 166 us -> 158 us  [grouped_body(): pl.pallas_call(functools.partial(fused_kernel, planes), out_shape=jax.Sha...]
where the time goes in v2:
time: 161 us
  Pallas kernels  158 us (98%)
  local copies, waits for them, and re-layouts  2.67 us (2%)
    pallas_call x1, Pallas kernels, grouped_body(): pl.pallas_call(functools.partial(fused_kernel, planes), out_shape=jax.Sha...  158 us

profile of v2, /device:TPU:1, one launch (start us, length us, event | category | flops | bytes accessed | tf_op | source)
XLA Modules:
  0.0 160.8 jit_solution(9331513579704049843)
XLA Ops:
  0.0 158.2 %shard_map.118 = bf16[768,1024]{1,0:T(8,128)(2,1)} custom-call(bf16[768,2048]{1,0:T(8,128)(2,1)} %tok_hbm.1, f32[128,2560]{1,0:T(8,128)} %gate_hbm.1, f32[128,2560]{1,0:T(8,128)} %value_hbm.1, f32[2560,128]{1,0:T(8,128)} %down_hbm.1, f32[1,2048]{1,0:T(1,128)} %bitcast.10, f32[20,128]{1,0:T(8,128)} %bitcast.6, f32[20,128]{1,0:T(8,128)} %bitcast.7, ...), custom_call_target="tpu_custom_call" | custom-call | tf_op jit(solution)/shard_map/pallas_call | solution.py:890
  158.2 2.7 %copy.14 = bf16[768,1024]{1,0:T(8,128)(2,1)} copy(bf16[768,1024]{1,0:T(8,128)(2,1)} %shard_map.118) | data formatting | bytes 3145728

commit v3 on v2

--- a/solution.py
+++ b/solution.py
@@ -87,14 +87,14 @@
     gate_hbm,
     value_hbm,
     down_hbm,
-    gain,
-    gate_scale,
-    value_scale,
-    gate_kernel,
-    value_kernel,
-    gate_bias,
-    value_bias,
-    osc,
+    gain_hbm,
+    gate_scale_hbm,
+    value_scale_hbm,
+    gate_kernel_hbm,
+    value_kernel_hbm,
+    gate_bias_hbm,
+    value_bias_hbm,
+    osc_hbm,
     out,
     tok,
     up_all,
@@ -114,6 +114,14 @@
     raw_gate,
     raw_value,
     raw_down,
+    gain,
+    gate_scale,
+    value_scale,
+    gate_kernel,
+    value_kernel,
+    gate_bias,
+    value_bias,
+    osc,
     sem_fetch,
     sem_own,
     sem_plane_send,
@@ -126,7 +134,8 @@
     sem_far_recv,
     sem_down_send,
     sem_down_recv,
-    sem_edge,
+    sem_edge_send,
+    sem_edge_recv,
     sem_tok_send,
     sem_tok_recv,
     sem_diag_send,
@@ -169,7 +178,20 @@
     fetches = [
         pltpu.make_async_copy(src, dst, sem_fetch.at[i])
         for i, (src, dst) in enumerate(
-            ((gate_hbm, raw_gate), (value_hbm, raw_value), (tok_hbm, raw_tok), (down_hbm, raw_down))
+            (
+                (gate_hbm, raw_gate),
+                (value_hbm, raw_value),
+                (tok_hbm, raw_tok),
+                (down_hbm, raw_down),
+                (gain_hbm, gain),
+                (gate_scale_hbm, gate_scale),
+                (value_scale_hbm, value_scale),
+                (gate_kernel_hbm, gate_kernel),
+                (value_kernel_hbm, value_kernel),
+                (gate_bias_hbm, gate_bias),
+                (value_bias_hbm, value_bias),
+                (osc_hbm, osc),
+            )
         )
     ]
     for fetch in fetches:
@@ -207,7 +229,7 @@
         return remote(
             wu.at[flip(mask), first:last],
             up_all.at[first:last, rows_of(me), :],
-            sem_plane_send.at[g, mask],
+            sem_plane_send.at[0],
             sem_plane_recv.at[g, mask],
             chip(flip(mask)),
         )
@@ -215,49 +237,45 @@
     def plane_up_landed(g, mask):
         first, last = groups[g]
         here = up_all.at[first:last, rows_of(z * GROUP + flip(mask)), :]
-        remote(here, here, sem_plane_send.at[g, mask], sem_plane_recv.at[g, mask], chip(flip(mask))).wait_recv()
+        remote(here, here, sem_plane_send.at[0], sem_plane_recv.at[g, mask], chip(flip(mask))).wait_recv()
 
     def first_hop(side, g, mask):
         first, last = groups[g]
         there = up_all.at[first:last, rows_of(z * GROUP + flip(mask)), :]
         here = there if mask else wu.at[p, first:last]
-        return remote(here, there, sem_first_send.at[side, g, mask], sem_first_recv.at[side, g, mask], line(side))
-
-    def first_landed(side, g, mask):
-        first, last = groups[g]
-        q = z + (2 * side - 1)
-        here = up_all.at[first:last, rows_of(q * GROUP + flip(mask)), :]
-        remote(
-            here, here, sem_first_send.at[side, g, mask], sem_first_recv.at[side, g, mask], (me, 1 - core)
-        ).wait_recv()
+        return remote(here, there, sem_first_send.at[side], sem_first_recv.at[side, mask], line(side))
+
+    def first_landed(side, mask):
+        here = up_all.at[:, rows_of((z + (2 * side - 1)) * GROUP + flip(mask)), :]
+        remote(here, here, sem_first_send.at[side], sem_first_recv.at[side, mask], (me, 1 - core)).wait_recv()
 
     def piece_hop(side, mask):
         here = up_all.at[:, rows_of((z + (2 * side - 1)) * GROUP + flip(mask)), :]
-        return remote(here, here, sem_piece_send.at[mask], sem_piece_recv.at[mask], line(side))
+        return remote(here, here, sem_piece_send.at[0], sem_piece_recv.at[mask], line(side))
 
     def piece_landed(side, mask):
         here = up_all.at[:, rows_of((z + 2 * (2 * side - 1)) * GROUP + flip(mask)), :]
-        remote(here, here, sem_piece_send.at[mask], sem_piece_recv.at[mask], (me, 1 - core)).wait_recv()
+        remote(here, here, sem_piece_send.at[0], sem_piece_recv.at[mask], (me, 1 - core)).wait_recv()
 
     def far_hop(side, distance, j):
         q = z + distance * (2 * side - 1)
         here = up_all.at[j, rows_of(q * GROUP, GROUP), :]
         return remote(
-            here, here, sem_far_send.at[side, distance - 1, j], sem_far_recv.at[side, distance - 1, j], line(side)
+            here, here, sem_far_send.at[side, distance - 1], sem_far_recv.at[side, distance - 1, j], line(side)
         )
 
     def far_landed(side, distance, j):
         q = z + distance * (2 * side - 1)
         here = up_all.at[j, rows_of(q * GROUP, GROUP), :]
         remote(
-            here, here, sem_far_send.at[side, distance - 2, j], sem_far_recv.at[side, distance - 2, j], (me, 1 - core)
+            here, here, sem_far_send.at[side, distance - 2], sem_far_recv.at[side, distance - 2, j], (me, 1 - core)
         ).wait_recv()
 
     def plane_down(mask):
         return remote(
             wd.at[flip(mask)],
             down_block(me),
-            sem_plane_send.at[2, mask],
+            sem_plane_send.at[1],
             sem_down_recv.at[me],
             chip(flip(mask)),
         )
@@ -270,7 +288,7 @@
 
     def wait_down(f):
         here = down_block(f)
-        remote(here, here, sem_down_send.at[f], sem_down_recv.at[f], (me, 1 - core)).wait_recv()
+        remote(here, here, sem_down_send.at[0], sem_down_recv.at[f], (me, 1 - core)).wait_recv()
 
     def both_ways(copy_of):
         @pl.when(has_up)
@@ -311,10 +329,10 @@
 
     def edge_copy(mask):
         here = edge_slot(p + 1)
-        return remote(here, here, sem_edge.at[0, mask], sem_edge.at[1, mask], chip(flip(mask)))
+        return remote(here, here, sem_edge_send.at[0], sem_edge_recv.at[mask], chip(flip(mask)))
 
     edge_next = remote(
-        edge_slot(GROUP), edge_slot(0), sem_edge.at[0, 0], sem_edge.at[1, 0], (me + GROUP, core)
+        edge_slot(GROUP), edge_slot(0), sem_edge_send.at[1], sem_edge_recv.at[0], (me + GROUP, core)
     )
 
     @pl.when(jnp.logical_not(has_down))
@@ -322,6 +340,7 @@
         edge[0:EDGE, :] = jnp.zeros_like(edge[0:EDGE, :])
 
     fetches[2].wait()
+    fetches[4].wait()
     edge[pl.ds(pl.multiple_of((p + 1) * EDGE, EDGE), EDGE), :] = normed(rows_own - EDGE, EDGE)
     for mask in others:
         edge_copy(mask).start()
@@ -348,29 +367,30 @@
 
     def token_copy(mask, part):
         here = token_rows(p, core, part)
-        return remote(here, here, sem_tok_send.at[mask - 1, part], sem_tok_recv.at[mask - 1, part], chip(flip(mask)))
+        return remote(here, here, sem_tok_send.at[0], sem_tok_recv.at[mask - 1, part], chip(flip(mask)))
 
     def token_relay(mask, part):
         here = diag_part(flip(mask), part, mask - 1)
         return remote(
             here,
             here,
-            sem_diag_send.at[mask - 1, part],
-            sem_diag_recv.at[mask - 1, part],
+            sem_diag_send.at[0],
+            sem_diag_recv.at[0],
             chip(flip(3 - mask)),
         )
 
     def token_pair(mask, part):
         here = token_rows(flip(mask), core, part)
         return remote(
-            here, here, sem_tok_pair_send.at[mask - 1, part], sem_tok_pair_recv.at[mask - 1, part], (me, 1 - core)
+            here, here, sem_tok_pair_send.at[0], sem_tok_pair_recv.at[mask - 1], (me, 1 - core)
         )
 
     for part in range(parts):
         for mask in (1, 2):
             token_copy(mask, part).start()
 
-    fetches[3].wait()
+    for i in (3, 5, 6, 7, 8, 9, 10, 11):
+        fetches[i].wait()
     for m in range(GROUP):
         wd[m] = raw_down[m * units : (m + 1) * units, :].astype(jnp.bfloat16)
     own_down.start()
@@ -391,7 +411,7 @@
 
     for mask in others:
         here = edge_slot(flip(mask) + 1)
-        remote(here, here, sem_edge.at[0, mask], sem_edge.at[1, mask], (me, 1 - core)).wait_recv()
+        remote(here, here, sem_edge_send.at[0], sem_edge_recv.at[mask], (me, 1 - core)).wait_recv()
 
     @pl.when(has_up)
     def _():
@@ -421,13 +441,14 @@
 
     def landed(mask, part):
         here = token_rows(flip(mask), core, part)
-        remote(here, here, sem_tok_send.at[mask - 1, part], sem_tok_recv.at[mask - 1, part], (me, 1 - core)).wait_recv()
-
-    def pair_landed(mask, part):
-        there = token_rows(flip(mask), 1 - core, part)
-        remote(
-            there, there, sem_tok_pair_send.at[mask - 1, part], sem_tok_pair_recv.at[mask - 1, part], (me, 1 - core)
-        ).wait_recv()
+        remote(here, here, sem_tok_send.at[0], sem_tok_recv.at[mask - 1, part], (me, 1 - core)).wait_recv()
+
+    def half_group(owner, side):
+        return tok.at[pl.ds(pl.multiple_of(owner * rows_own + side * part_rows, part_rows), part_rows), :]
+
+    def pair_landed(mask):
+        there = half_group(flip(mask), 1 - core)
+        remote(there, there, sem_tok_pair_send.at[0], sem_tok_pair_recv.at[mask - 1], (me, 1 - core)).wait_recv()
 
     def pass_tokens(part):
         for mask in (1, 2):
@@ -438,14 +459,12 @@
     def near(side):
         def pieces():
             for mask in range(GROUP):
-                for g in range(2):
-                    first_landed(side, g, mask)
+                first_landed(side, mask)
                 piece_hop(side, mask).start()
 
         def whole():
             for mask in range(GROUP):
-                for g in range(2):
-                    first_landed(side, g, mask)
+                first_landed(side, mask)
 
         onward = z + (1 - 2 * side)
         into_end = onward == (planes - 1 if side == 0 else 0)
@@ -503,7 +522,7 @@
     @pl.when(has_down)
     def _():
         here = edge_slot(0)
-        remote(here, here, sem_edge.at[0, 0], sem_edge.at[1, 0], (me, 1 - core)).wait_recv()
+        remote(here, here, sem_edge_send.at[1], sem_edge_recv.at[0], (me, 1 - core)).wait_recv()
 
     own_up.wait()
     own_down.wait()
@@ -542,7 +561,7 @@
         return remote(
             stage.at[c, owner],
             pair_in.at[c % per_core, owner],
-            sem_pair_send.at[c % per_core, owner],
+            sem_pair_send.at[0],
             sem_pair_recv.at[c % per_core, owner],
             (me, 1 - core),
         )
@@ -553,12 +572,11 @@
         return pl.ds(pl.multiple_of(which * half_rows, half_rows), half_rows)
 
     def peer_copy(c, mask, which):
-        slot = (mask - 1) * 2 + which
         return remote(
             stage.at[c, flip(mask), half_of(which)],
             peer_in.at[c % per_core, mask - 1, half_of(which)],
-            sem_peer_send.at[c % per_core, slot],
-            sem_peer_recv.at[c % per_core, slot],
+            sem_peer_send.at[0],
+            sem_peer_recv.at[c % per_core],
             chip(flip(mask)),
         )
 
@@ -566,7 +584,7 @@
         return remote(
             stage.at[c, flip(3), half_of(mask - 1)],
             relay_in.at[c % per_core, mask - 1],
-            sem_relay_send.at[c % per_core, mask - 1],
+            sem_relay_send.at[0],
             sem_relay_recv.at[c % per_core, mask - 1],
             chip(flip(mask)),
         )
@@ -612,11 +630,11 @@
         return c // per_core == core
 
     def own_down_out():
-        both_ways(lambda side: line_down(side, me, me if side == 0 else planes * GROUP + p, wd.at[p]))
+        both_ways(lambda side: line_down(side, me, side, wd.at[p]))
         for mask in others:
             f = z * GROUP + flip(mask)
             wait_down(f)
-            both_ways(lambda side: line_down(side, f, f if side == 0 else planes * GROUP + flip(mask)))
+            both_ways(lambda side: line_down(side, f, side))
 
     diag_round = jnp.where(inner_plane, blocks - 1, min(2, blocks - 1))
 
@@ -634,16 +652,9 @@
 
         @pl.when(j == diag_round)
         def _():
+            here = half_group(flip(3), core)
+            remote(here, here, sem_diag_send.at[0], sem_diag_recv.at[0], (me, 1 - core)).wait_recv()
             for part in range(parts):
-                for which in (0, 1):
-                    here = diag_part(flip(3), part, which)
-                    remote(
-                        here,
-                        here,
-                        sem_diag_send.at[which, part],
-                        sem_diag_recv.at[which, part],
-                        (me, 1 - core),
-                    ).wait_recv()
                 token_pair(3, part).start()
 
         final = j == blocks - 1
@@ -658,8 +669,7 @@
 
             @pl.when((mask > 0) & (j == ready))
             def _():
-                for part in range(parts):
-                    pair_landed(mask, part)
+                pair_landed(mask)
 
             first = jnp.where(j == ready, 0, j)
             last = jnp.where(j >= ready, j + 1, 0)
@@ -672,14 +682,14 @@
 
             @pl.when(final)
             def _():
-                for n in range(strips):
-                    product(z * strips + n, flip(mask))
-
                 @pl.when(mine(z * strips) & (i > 0))
                 def _():
                     for n in range(strips):
                         send_out(z * strips + n, mask + 1)
 
+                for n in range(strips):
+                    product(z * strips + n, flip(mask))
+
             return inner
 
         return lax.fori_loop(0, GROUP, group, carry)
@@ -704,28 +714,27 @@
 
                 @pl.when((below == 1) & has_up)
                 def _():
-                    line_down(0, f, f).start()
+                    line_down(0, f, 2 + q).start()
 
                 @pl.when((below == 0) & has_down)
                 def _():
-                    line_down(1, f, f).start()
+                    line_down(1, f, 2 + q).start()
 
                 return carry
 
             lax.fori_loop(0, GROUP, one, 0)
 
+    def sent(here, send, recv):
+        remote(here, here, send, recv, (me, 1 - core)).wait_send()
+
     def drain_early():
-        for part in range(parts):
-            for mask in (1, 2):
-                token_copy(mask, part).wait_send()
-                token_relay(mask, part).wait_send()
-            for mask in others:
-                token_pair(mask, part).wait_send()
-        for mask in others:
-            edge_copy(mask).wait_send()
-            plane_down(mask).wait_send()
-            for g in range(2):
-                plane_up(g, mask).wait_send()
+        sent(tok.at[0:rows_own], sem_tok_send.at[0], sem_tok_recv.at[0, 0])
+        sent(tok.at[0:part_rows], sem_diag_send.at[0], sem_diag_recv.at[0])
+        sent(tok.at[0 : 3 * part_rows], sem_tok_pair_send.at[0], sem_tok_pair_recv.at[0])
+        sent(edge.at[0 : 3 * EDGE], sem_edge_send.at[0], sem_edge_recv.at[0])
+        sent(wu.at[0:3], sem_plane_send.at[0], sem_plane_recv.at[0, 0])
+        sent(wd.at[0:3], sem_plane_send.at[1], sem_plane_recv.at[0, 0])
+        whole = up_all.at[:, rows_of(0, GROUP), :]
 
         @pl.when(has_up)
         def _():
@@ -735,17 +744,14 @@
 
             @pl.when(has_up if side == 0 else has_down)
             def _():
-                for g in range(2):
-                    for mask in range(GROUP):
-                        first_hop(side, g, mask).wait_send()
+                sent(whole, sem_first_send.at[side], sem_first_recv.at[side, 0])
 
             onward = z + (1 - 2 * side)
             into_end = onward == (planes - 1 if side == 0 else 0)
 
             @pl.when(inner_plane & into_end)
             def _():
-                for mask in range(GROUP):
-                    piece_hop(side, mask).wait_send()
+                sent(whole, sem_piece_send.at[0], sem_piece_recv.at[0])
 
             @pl.when(inner_plane)
             def _():
@@ -754,11 +760,7 @@
 
                     @pl.when(valid & (jnp.logical_not(into_end) if distance == 1 else True))
                     def _():
-                        def one(j, carry):
-                            far_hop(side, distance, j).wait_send()
-                            return carry
-
-                        lax.fori_loop(0, blocks, one, 0)
+                        sent(whole, sem_far_send.at[side, distance - 1], sem_far_recv.at[side, 0, 0])
 
     def down_step(n, before):
         step = n // strips
@@ -816,9 +818,9 @@
     def finish(c):
         i = c % per_core
         total = stage[c, p].astype(jnp.float32)
+        landed_all = peer_in.at[i]
+        remote(landed_all, landed_all, sem_peer_send.at[0], sem_peer_recv.at[i], chip(flip(1))).wait_recv()
         for mask in (1, 2):
-            for which in (0, 1):
-                peer_copy(c, mask, which).wait_recv()
             total = total + peer_in[i, mask - 1].astype(jnp.float32)
         cols = pl.ds(pl.multiple_of(i * strip, strip), strip)
         out[:, cols] = (total * osc[0:1, cols]).astype(jnp.bfloat16)
@@ -833,42 +835,25 @@
 
     lax.fori_loop(0, per_core, finish_one, 0)
 
-    def drain_out(i, carry):
-        for mask in (1, 2):
-            relay_copy(core * per_core + i, mask).wait_send()
-            for which in (0, 1):
-                peer_copy(core * per_core + i, mask, which).wait_send()
-
-        def one(owner, inner):
-            pair_copy((1 - core) * per_core + i, owner).wait_send()
-            return inner
-
-        return lax.fori_loop(0, GROUP, one, carry)
-
-    lax.fori_loop(0, per_core, drain_out, 0)
-
+    sent(pair_in, sem_pair_send.at[0], sem_pair_recv.at[0, 0])
+    sent(peer_in, sem_peer_send.at[0], sem_peer_recv.at[0])
+    sent(relay_in, sem_relay_send.at[0], sem_relay_recv.at[0, 0])
     for side in (0, 1):
 
         @pl.when(has_up if side == 0 else has_down)
         def _():
-            for mask in range(GROUP):
-                f = z * GROUP + flip(mask)
-                line_down(side, f, f if side == 0 else planes * GROUP + flip(mask)).wait_send()
+            sent(down_all.at[0], sem_down_send.at[side], sem_down_recv.at[0])
 
     @pl.when(inner_plane)
     def _():
-        def drain_down(f, carry):
-            @pl.when(f // GROUP < z)
+        def drain_down(q, carry):
+            @pl.when(q != z)
             def _():
-                line_down(0, f, f).wait_send()
-
-            @pl.when(f // GROUP > z)
-            def _():
-                line_down(1, f, f).wait_send()
+                sent(down_all.at[0], sem_down_send.at[2 + q], sem_down_recv.at[0])
 
             return carry
 
-        lax.fori_loop(0, planes * GROUP, drain_down, 0)
+        lax.fori_loop(0, planes, drain_down, 0)
 
 
 def grouped_body(count, tokens, norm_gain, gate_weight, value_weight, gate_scale, value_scale, gate_kernel, value_kernel, gate_bias, value_bias, down_weight, down_scale):
@@ -890,7 +875,7 @@
     return pl.pallas_call(
         functools.partial(fused_kernel, planes),
         out_shape=jax.ShapeDtypeStruct((rows, half * chunk), bf16),
-        in_specs=[hbm] * 4 + [vmem] * 8,
+        in_specs=[hbm] * 12,
         out_specs=vmem,
         scratch_shapes=[
             pltpu.VMEM((GROUP * rows, width), bf16),
@@ -911,30 +896,39 @@
             pltpu.VMEM((piece, local), f32),
             pltpu.VMEM((piece, local), f32),
             pltpu.VMEM((local, out_piece), f32),
-            dma((4,)),
+            pltpu.VMEM((1, width), f32),
+            pltpu.VMEM((local // 128, 128), f32),
+            pltpu.VMEM((local // 128, 128), f32),
+            pltpu.VMEM(gate_kernel.shape, f32),
+            pltpu.VMEM(value_kernel.shape, f32),
+            pltpu.VMEM((local // 128, 128), f32),
+            pltpu.VMEM((local // 128, 128), f32),
+            pltpu.VMEM((1, half * chunk), f32),
+            dma((12,)),
             dma((2,)),
-            dma((3, GROUP)),
+            dma((2,)),
             dma((2, GROUP)),
-            dma((2, 2, GROUP)),
-            dma((2, 2, GROUP)),
+            dma((2,)),
+            dma((2, GROUP)),
+            dma((1,)),
             dma((GROUP,)),
+            dma((2, max(1, planes - 2))),
+            dma((2, max(1, planes - 2), blocks)),
+            dma((2 + planes,)),
+            dma((count,)),
+            dma((2,)),
             dma((GROUP,)),
-            dma((2, max(1, planes - 2), blocks)),
-            dma((2, max(1, planes - 2), blocks)),
-            dma((count + GROUP,)),
-            dma((count,)),
-            dma((2, GROUP)),
+            dma((1,)),
             dma((2, 2)),
-            dma((2, 2)),
-            dma((2, 2)),
-            dma((2, 2)),
-            dma((3, 2)),
-            dma((3, 2)),
+            dma((1,)),
+            dma((1,)),
+            dma((1,)),
+            dma((3,)),
+            dma((1,)),
             dma((per_core, GROUP)),
-            dma((per_core, GROUP)),
-            dma((per_core, 4)),
-            dma((per_core, 4)),
-            dma((per_core, 2)),
+            dma((1,)),
+            dma((per_core,)),
+            dma((1,)),
             dma((per_core, 2)),
         ],
         compiler_params=pltpu.CompilerParams(

time: 161 us -> 157 us (0.975)
  Pallas kernels: 158 us -> 154 us
    pallas_call x1, Pallas kernels: 158 us -> 154 us  [grouped_body(): pl.pallas_call(functools.partial(fused_kernel, planes), out_shape=jax.Sha...]
where the time goes in v3:
time: 157 us
  Pallas kernels  154 us (98%)
  local copies, waits for them, and re-layouts  2.67 us (2%)
    pallas_call x1, Pallas kernels, grouped_body(): pl.pallas_call(functools.partial(fused_kernel, planes), out_shape=jax.Sha...  154 us

profile of v3, /device:TPU:1, one launch (start us, length us, event | category | flops | bytes accessed | tf_op | source)
XLA Modules:
  0.0 156.9 jit_solution(17457196253732574718)
XLA Ops:
  0.0 154.2 %shard_map.118 = bf16[768,1024]{1,0:T(8,128)(2,1)} custom-call(bf16[768,2048]{1,0:T(8,128)(2,1)} %tok_hbm.1, f32[128,2560]{1,0:T(8,128)} %gate_hbm.1, f32[128,2560]{1,0:T(8,128)} %value_hbm.1, f32[2560,128]{1,0:T(8,128)} %down_hbm.1, f32[1,2048]{1,0:T(1,128)} %bitcast.10, f32[20,128]{1,0:T(8,128)} %bitcast.6, f32[20,128]{1,0:T(8,128)} %bitcast.7, ...), custom_call_target="tpu_custom_call" | custom-call | tf_op jit(solution)/shard_map/pallas_call | solution.py:875
  154.2 2.7 %copy.14 = bf16[768,1024]{1,0:T(8,128)(2,1)} copy(bf16[768,1024]{1,0:T(8,128)(2,1)} %shard_map.118) | data formatting | bytes 3145728

commit v4 on v3

--- a/solution.py
+++ b/solution.py
@@ -110,10 +110,10 @@
     par,
     wu,
     wd,
-    raw_tok,
     raw_gate,
     raw_value,
     raw_down,
+    begun_sum,
     gain,
     gate_scale,
     value_scale,
@@ -154,7 +154,7 @@
     me = lax.axis_index("fs")
     core = lax.axis_index("tp")
     z, p = me // GROUP, me % GROUP
-    rows_own = raw_tok.shape[0]
+    rows_own = tok.shape[0] // GROUP
     part_rows = rows_own // 2
     blocks, piece = wu.shape[1], wu.shape[2]
     units = hidden.shape[1]
@@ -175,13 +175,14 @@
 
     others = (1, 2, 3)
 
+    own_rows = pl.ds(pl.multiple_of(p * rows_own, rows_own), rows_own)
     fetches = [
         pltpu.make_async_copy(src, dst, sem_fetch.at[i])
         for i, (src, dst) in enumerate(
             (
                 (gate_hbm, raw_gate),
                 (value_hbm, raw_value),
-                (tok_hbm, raw_tok),
+                (tok_hbm, tok.at[own_rows, :]),
                 (down_hbm, raw_down),
                 (gain_hbm, gain),
                 (gate_scale_hbm, gate_scale),
@@ -309,16 +310,18 @@
             wu[m, j, :, 128:256] = raw_value[:, first : first + 128].astype(jnp.bfloat16)
 
     def normed(first, count):
-        values = raw_tok[pl.ds(first, count), :].astype(jnp.float32)
+        start = pl.multiple_of(p * rows_own + first, count)
+        values = tok[pl.ds(start, count), :].astype(jnp.float32)
         scaled = values * lax.rsqrt(jnp.mean(values * values, axis=1, keepdims=True) + epsilon)
         return (scaled * gain[...]).astype(jnp.bfloat16)
 
     fetches[0].wait()
     fetches[1].wait()
-    for j in range(blocks):
-        cast_block(j)
-    pl.semaphore_wait(barrier, 4 + has_up.astype(jnp.int32) + has_down.astype(jnp.int32))
     for g in range(2):
+        for j in range(*groups[g]):
+            cast_block(j)
+        if g == 0:
+            pl.semaphore_wait(barrier, 4 + has_up.astype(jnp.int32) + has_down.astype(jnp.int32))
         for mask in others:
             plane_up(g, mask).start()
         both_ways(lambda side: first_hop(side, g, 0))
@@ -427,9 +430,25 @@
     def wide(j):
         return pl.ds(pl.multiple_of(j * 256, 256), 256)
 
-    def unit(owner, j):
+    plane_rows = GROUP * piece
+    near_part = pl.ds(pl.multiple_of(jnp.where(has_down, plane_rows, 0), plane_rows), (planes - 1) * plane_rows)
+    far_part = pl.ds(pl.multiple_of(jnp.where(has_down, 0, (planes - 1) * plane_rows), plane_rows), plane_rows)
+
+    def begin(owner, j, slot):
         rows = pl.ds(pl.multiple_of(owner * rows_own, rows_own), rows_own)
-        taps[8:, :] = jnp.dot(tok[rows, :], up_all[j], preferred_element_type=jnp.float32)
+        begun_sum[slot] = jnp.dot(tok[rows, near_part], up_all[j, near_part, :], preferred_element_type=jnp.float32)
+
+    def begin_own(j, carry):
+        begin(p, j, j)
+        return carry
+
+    def unit(owner, j, slot=None):
+        rows = pl.ds(pl.multiple_of(owner * rows_own, rows_own), rows_own)
+        if slot is not None:
+            rest = jnp.dot(tok[rows, far_part], up_all[j, far_part, :], preferred_element_type=jnp.float32)
+            taps[8:, :] = begun_sum[slot] + rest
+        else:
+            taps[8:, :] = jnp.dot(tok[rows, :], up_all[j], preferred_element_type=jnp.float32)
         taps[0:8, :] = edge_pre[j, pl.ds(pl.multiple_of(owner * EDGE + EDGE - 8, 8), 8), :]
         conv = par[4:5, wide(j)] + par[3:4, wide(j)] * taps[8 : 8 + rows_own, :]
         conv = conv + par[2:3, wide(j)] * taps[7 : 7 + rows_own, :]
@@ -527,6 +546,11 @@
     own_up.wait()
     own_down.wait()
 
+    @pl.when(end_plane)
+    def _():
+        lax.fori_loop(0, blocks, begin_own, 0)
+
+
     def edge_block(j):
         ahead = jnp.dot(edge[0 : GROUP * EDGE, :], up_all[j], preferred_element_type=jnp.float32)
         edge_pre[j] = ahead
@@ -541,6 +565,9 @@
                     def _():
                         far_landed(side, distance, j)
                         far_hop(side, distance, j).start()
+
+            edge_block(j)
+            unit(p, j)
 
             @pl.when(j == max(0, blocks - 2))
             def _():
@@ -639,17 +666,6 @@
     diag_round = jnp.where(inner_plane, blocks - 1, min(2, blocks - 1))
 
     def up_round(j, carry):
-        @pl.when(end_plane)
-        def _():
-            for distance in range(3, planes):
-                for side in (0, 1):
-
-                    @pl.when((z >= distance) if side == 0 else (z < planes - distance))
-                    def _():
-                        far_landed(side, distance, j)
-
-        edge_block(j)
-
         @pl.when(j == diag_round)
         def _():
             here = half_group(flip(3), core)
@@ -657,16 +673,30 @@
             for part in range(parts):
                 token_pair(3, part).start()
 
+        @pl.when(end_plane & (j > 0) & (j < 3) & (blocks > 4))
+        def _():
+            for k in (blocks - 2, blocks - 1):
+                begin(flip(j), k, 2 * j + k)
+
+        @pl.when(end_plane)
+        def _():
+            for distance in range(3, planes):
+                for side in (0, 1):
+
+                    @pl.when((z >= distance) if side == 0 else (z < planes - distance))
+                    def _():
+                        far_landed(side, distance, j)
+
+        @pl.when(end_plane)
+        def _():
+            edge_block(j)
+
         final = j == blocks - 1
 
         def group(i, inner):
             mask = jnp.where(final, 3 - i, i)
             ready = jnp.where(mask == 3, diag_round, 0)
 
-            @pl.when((mask == 3) & (j == diag_round))
-            def _():
-                own_down_out()
-
             @pl.when((mask > 0) & (j == ready))
             def _():
                 pair_landed(mask)
@@ -674,32 +704,47 @@
             first = jnp.where(j == ready, 0, j)
             last = jnp.where(j >= ready, j + 1, 0)
 
+            begun = end_plane & ((mask == 0) | ((mask < 3) & (j >= blocks - 2) & (blocks > 4)))
+
             def one(k, deeper):
                 unit(flip(mask), k)
                 return deeper
 
-            lax.fori_loop(first, last, one, inner)
+            lax.fori_loop(first, jnp.where(mask == 0, first, jnp.where(begun, first, last)), one, inner)
+
+            @pl.when(inner_plane & (mask == 3) & (j == diag_round))
+            def _():
+                own_down_out()
+
+            @pl.when(begun)
+            def _():
+                unit(flip(mask), j, jnp.where(mask == 0, j, 2 * mask + j))
+
 
             @pl.when(final)
             def _():
-                @pl.when(mine(z * strips) & (i > 0))
+                for n in range(strips):
+                    product(z * strips + n, flip(mask))
+
+                @pl.when(mine(z * strips))
                 def _():
                     for n in range(strips):
-                        send_out(z * strips + n, mask + 1)
-
-                for n in range(strips):
-                    product(z * strips + n, flip(mask))
+                        send_out(z * strips + n, mask)
 
             return inner
 
-        return lax.fori_loop(0, GROUP, group, carry)
+        lax.fori_loop(0, GROUP, group, carry)
+
+        @pl.when(end_plane & (j == diag_round))
+        def _():
+            own_down_out()
+
+        return carry
 
     lax.fori_loop(0, blocks, up_round, 0)
 
     @pl.when(mine(z * strips))
     def _():
-        for n in range(strips):
-            send_out(z * strips + n, 0)
         for n in range(strips - 1):
             pass_on(z * strips + n)
 
@@ -772,6 +817,9 @@
         @pl.when((n == strips) & inner_plane)
         def _():
             pass_plane(1)
+
+        @pl.when((n == strips + 1) & inner_plane)
+        def _():
             pass_plane(2)
 
         @pl.when(n == 2 * strips)
@@ -874,7 +922,7 @@
     hbm = pl.BlockSpec(memory_space=pl.ANY)
     return pl.pallas_call(
         functools.partial(fused_kernel, planes),
-        out_shape=jax.ShapeDtypeStruct((rows, half * chunk), bf16),
+        out_shape=pltpu.VMEM((rows, half * chunk), bf16),
         in_specs=[hbm] * 12,
         out_specs=vmem,
         scratch_shapes=[
@@ -892,10 +940,10 @@
             pltpu.VMEM((8, 2 * units), f32),
             pltpu.VMEM((GROUP, blocks, piece, 256), bf16),
             pltpu.VMEM((GROUP, units, out_piece), bf16),
-            pltpu.VMEM((rows, width), bf16),
             pltpu.VMEM((piece, local), f32),
             pltpu.VMEM((piece, local), f32),
             pltpu.VMEM((local, out_piece), f32),
+            pltpu.VMEM((blocks + 4, rows, 256), f32),
             pltpu.VMEM((1, width), f32),
             pltpu.VMEM((local // 128, 128), f32),
             pltpu.VMEM((local // 128, 128), f32),
@@ -932,7 +980,7 @@
             dma((per_core, 2)),
         ],
         compiler_params=pltpu.CompilerParams(
-            collective_id=0, has_side_effects=True, vmem_limit_bytes=67043328
+            collective_id=0, has_side_effects=True, vmem_limit_bytes=65400000
         ),
     )(
         tokens,

time: 157 us -> 152 us (0.968)
  Pallas kernels: 154 us -> 151 us
    pallas_call x1, Pallas kernels: 154 us -> 151 us  [grouped_body(): pl.pallas_call(functools.partial(fused_kernel, planes), out_shape=pltpu.V...]
where the time goes in v4:
time: 152 us
  Pallas kernels  151 us (99%)
    pallas_call x1, Pallas kernels, grouped_body(): pl.pallas_call(functools.partial(fused_kernel, planes), out_shape=pltpu.V...  151 us

profile of v4, /device:TPU:1, one launch (start us, length us, event | category | flops | bytes accessed | tf_op | source)
XLA Modules:
  0.0 151.7 jit_solution(17372422412210837663)
XLA Ops:
  0.0 150.5 %shard_map.118 = bf16[768,1024]{1,0:T(8,128)(2,1)S(1)} custom-call(bf16[768,2048]{1,0:T(8,128)(2,1)} %tok_hbm.1, f32[128,2560]{1,0:T(8,128)} %gate_hbm.1, f32[128,2560]{1,0:T(8,128)} %value_hbm.1, f32[2560,128]{1,0:T(8,128)} %down_hbm.1, f32[1,2048]{1,0:T(1,128)} %bitcast.10, f32[20,128]{1,0:T(8,128)} %bitcast.6, f32[20,128]{1,0:T(8,128)} %bitcast.7, ...), custom_call_target="tpu_custom_call" | custom-call | tf_op jit(solution)/shard_map/pallas_call | solution.py:923
  150.5 1.1 copy.14

commit v5 on v4

--- a/solution.py
+++ b/solution.py
@@ -104,6 +104,10 @@
     pair_in,
     peer_in,
     relay_in,
+    guest_in,
+    guest_sum,
+    guest_out,
+    guest_back,
     taps,
     edge,
     edge_pre,
@@ -148,6 +152,12 @@
     sem_peer_recv,
     sem_relay_send,
     sem_relay_recv,
+    sem_guest_send,
+    sem_guest_recv,
+    sem_swap_send,
+    sem_swap_recv,
+    sem_home_send,
+    sem_home_recv,
 ):
     planes = depth_planes
     half = planes // 2
@@ -593,28 +603,87 @@
             (me, 1 - core),
         )
 
-    half_rows = rows_own // 2
-
-    def half_of(which):
-        return pl.ds(pl.multiple_of(which * half_rows, half_rows), half_rows)
-
-    def peer_copy(c, mask, which):
+    slab = guest_in.shape[2]
+    kept = rows_own - slab
+    lends = end_plane & (z // half == core)
+    hosts = inner_plane & (((z == 1) & (core == 0)) | ((z == planes - 2) & ((planes - 1) // half == core)))
+    if planes < 4:
+        lends = hosts = me < 0
+
+    def sized(run):
+        @pl.when(lends)
+        def _():
+            run(kept // 2)
+
+        @pl.when(jnp.logical_not(lends))
+        def _():
+            run(rows_own // 2)
+
+    def half_of(which, size):
+        return pl.ds(pl.multiple_of(which * size, size), size)
+
+    def peer_copy(c, mask, which, size):
         return remote(
-            stage.at[c, flip(mask), half_of(which)],
-            peer_in.at[c % per_core, mask - 1, half_of(which)],
+            stage.at[c, flip(mask), half_of(which, size)],
+            peer_in.at[c % per_core, mask - 1, half_of(which, size)],
             sem_peer_send.at[0],
             sem_peer_recv.at[c % per_core],
             chip(flip(mask)),
         )
 
-    def relay_copy(c, mask):
+    def relay_copy(c, mask, size):
         return remote(
-            stage.at[c, flip(3), half_of(mask - 1)],
-            relay_in.at[c % per_core, mask - 1],
+            stage.at[c, flip(3), half_of(mask - 1, size)],
+            relay_in.at[c % per_core, mask - 1, 0:size],
             sem_relay_send.at[0],
             sem_relay_recv.at[c % per_core, mask - 1],
             chip(flip(mask)),
         )
+
+    def guest_copy(c):
+        return remote(
+            stage.at[c, :, kept:rows_own, :],
+            guest_in.at[c % per_core],
+            sem_guest_send.at[0],
+            sem_guest_recv.at[c % per_core],
+            (jnp.where(z == 0, me + GROUP, me - GROUP), core),
+        )
+
+    def guest_swap(k, mask):
+        return remote(
+            guest_in.at[k, flip(mask)],
+            guest_sum.at[k, mask - 1],
+            sem_swap_send.at[0],
+            sem_swap_recv.at[k],
+            chip(flip(mask)),
+        )
+
+    def guest_home(k):
+        return remote(
+            guest_out.at[k],
+            guest_back.at[k],
+            sem_home_send.at[0],
+            sem_home_recv.at[k],
+            (jnp.where(z == 1, me - GROUP, me + GROUP), core),
+        )
+
+    def landing(here, recv):
+        remote(here, here, sem_guest_send.at[0], recv, chip(flip(1))).wait_recv()
+
+    def swap_guests():
+        for k in range(per_core):
+            landing(guest_in.at[k], sem_guest_recv.at[k])
+            for mask in others:
+                guest_swap(k, mask).start()
+
+    def return_guests():
+        for k in range(per_core):
+            landing(guest_sum.at[k], sem_swap_recv.at[k])
+            total = guest_in[k, p].astype(jnp.float32)
+            for mask in others:
+                total = total + guest_sum[k, mask - 1].astype(jnp.float32)
+            guest_out[k] = (total * osc[0:1, k * strip : (k + 1) * strip]).astype(jnp.bfloat16)
+            guest_home(k).start()
 
     def combine(c, owner):
         pair_copy(c, owner).wait_recv()
@@ -637,21 +706,31 @@
 
         @pl.when(mask == 3)
         def _():
-            for way in (1, 2):
-                relay_copy(c, way).start()
+            def run(size):
+                for way in (1, 2):
+                    relay_copy(c, way, size).start()
+
+            sized(run)
 
         @pl.when((mask == 1) | (mask == 2))
         def _():
-            peer_copy(c, mask, mask - 1).start()
+            sized(lambda size: peer_copy(c, mask, mask - 1, size).start())
+
+        @pl.when((mask == 0) & lends)
+        def _():
+            guest_copy(c).start()
 
     def pass_on(c):
-        for mask in (1, 2):
-            relay_copy(c, mask).wait_recv()
-            owner = flip(3 - mask)
-            rows = half_of(mask - 1)
-            total = stage[c, owner, rows, :].astype(jnp.float32) + relay_in[c % per_core, mask - 1].astype(jnp.float32)
-            stage[c, owner, rows, :] = total.astype(jnp.bfloat16)
-            peer_copy(c, 3 - mask, mask - 1).start()
+        def run(size):
+            for mask in (1, 2):
+                relay_copy(c, mask, size).wait_recv()
+                owner = flip(3 - mask)
+                rows = half_of(mask - 1, size)
+                added = relay_in[c % per_core, mask - 1, 0:size].astype(jnp.float32)
+                stage[c, owner, rows, :] = (stage[c, owner, rows, :].astype(jnp.float32) + added).astype(jnp.bfloat16)
+                peer_copy(c, 3 - mask, mask - 1, size).start()
+
+        sized(run)
 
     def mine(c):
         return c // per_core == core
@@ -665,6 +744,8 @@
 
     diag_round = jnp.where(inner_plane, blocks - 1, min(2, blocks - 1))
 
+    down_unit = jnp.where(inner_plane, min(2, blocks - 1), 0)
+
     def up_round(j, carry):
         @pl.when(j == diag_round)
         def _():
@@ -675,8 +756,7 @@
 
         @pl.when(end_plane & (j > 0) & (j < 3) & (blocks > 4))
         def _():
-            for k in (blocks - 2, blocks - 1):
-                begin(flip(j), k, 2 * j + k)
+            begin(flip(j), blocks - 1, blocks + j - 1)
 
         @pl.when(end_plane)
         def _():
@@ -704,21 +784,22 @@
             first = jnp.where(j == ready, 0, j)
             last = jnp.where(j >= ready, j + 1, 0)
 
-            begun = end_plane & ((mask == 0) | ((mask < 3) & (j >= blocks - 2) & (blocks > 4)))
+            begun = end_plane & ((mask == 0) | ((mask < 3) & (j == blocks - 1) & (blocks > 4)))
 
             def one(k, deeper):
                 unit(flip(mask), k)
+
+                @pl.when((mask == 3) & (j == diag_round) & (k == down_unit))
+                def _():
+                    own_down_out()
+
                 return deeper
 
             lax.fori_loop(first, jnp.where(mask == 0, first, jnp.where(begun, first, last)), one, inner)
-
-            @pl.when(inner_plane & (mask == 3) & (j == diag_round))
-            def _():
-                own_down_out()
 
             @pl.when(begun)
             def _():
-                unit(flip(mask), j, jnp.where(mask == 0, j, 2 * mask + j))
+                unit(flip(mask), j, jnp.where(mask == 0, j, mask + j))
 
 
             @pl.when(final)
@@ -734,10 +815,6 @@
             return inner
 
         lax.fori_loop(0, GROUP, group, carry)
-
-        @pl.when(end_plane & (j == diag_round))
-        def _():
-            own_down_out()
 
         return carry
 
@@ -831,6 +908,10 @@
             for later in range(3, 2 * planes - 1):
                 pass_plane(later)
 
+            @pl.when(hosts)
+            def _():
+                swap_guests()
+
         @pl.when(valid & end_plane)
         def _():
             for i in range(GROUP // strips):
@@ -865,13 +946,22 @@
 
     def finish(c):
         i = c % per_core
-        total = stage[c, p].astype(jnp.float32)
-        landed_all = peer_in.at[i]
-        remote(landed_all, landed_all, sem_peer_send.at[0], sem_peer_recv.at[i], chip(flip(1))).wait_recv()
-        for mask in (1, 2):
-            total = total + peer_in[i, mask - 1].astype(jnp.float32)
         cols = pl.ds(pl.multiple_of(i * strip, strip), strip)
-        out[:, cols] = (total * osc[0:1, cols]).astype(jnp.bfloat16)
+
+        def run(size):
+            rows = 2 * size
+            landing(peer_in.at[i, :, 0:rows, :], sem_peer_recv.at[i])
+            total = stage[c, p, 0:rows].astype(jnp.float32)
+            for mask in (1, 2):
+                total = total + peer_in[i, mask - 1, 0:rows].astype(jnp.float32)
+            out[0:rows, cols] = (total * osc[0:1, cols]).astype(jnp.bfloat16)
+
+        sized(run)
+
+        @pl.when(lends)
+        def _():
+            landing(guest_back.at[i], sem_home_recv.at[i])
+            out[kept:rows_own, cols] = guest_back[i]
 
     @pl.when(last >= 0)
     def _():
@@ -881,11 +971,29 @@
         finish(core * per_core + i)
         return carry
 
+    @pl.when(hosts)
+    def _():
+        return_guests()
+
     lax.fori_loop(0, per_core, finish_one, 0)
 
     sent(pair_in, sem_pair_send.at[0], sem_pair_recv.at[0, 0])
-    sent(peer_in, sem_peer_send.at[0], sem_peer_recv.at[0])
-    sent(relay_in, sem_relay_send.at[0], sem_relay_recv.at[0, 0])
+
+    def drain_sums(size):
+        sent(peer_in.at[:, :, 0 : 2 * size, :], sem_peer_send.at[0], sem_peer_recv.at[0])
+        sent(relay_in.at[:, :, 0:size, :], sem_relay_send.at[0], sem_relay_recv.at[0, 0])
+
+    sized(drain_sums)
+
+    @pl.when(lends)
+    def _():
+        sent(guest_in, sem_guest_send.at[0], sem_guest_recv.at[0])
+
+    @pl.when(hosts)
+    def _():
+        sent(guest_sum, sem_swap_send.at[0], sem_swap_recv.at[0])
+        sent(guest_out, sem_home_send.at[0], sem_home_recv.at[0])
+
     for side in (0, 1):
 
         @pl.when(has_up if side == 0 else has_down)
@@ -916,6 +1024,7 @@
     strip = 2 * out_piece
     strips = chunk // strip
     per_core = half * strips
+    slab = max(1, rows // 8 // 32) * 32
     dma = pltpu.SemaphoreType.DMA
     bf16, f32 = jnp.bfloat16, jnp.float32
     vmem = pl.BlockSpec(memory_space=pltpu.VMEM)
@@ -934,6 +1043,10 @@
             pltpu.VMEM((per_core, GROUP, rows, strip), bf16),
             pltpu.VMEM((per_core, 2, rows, strip), bf16),
             pltpu.VMEM((per_core, 2, rows // 2, strip), bf16),
+            pltpu.VMEM((per_core, GROUP, slab, strip), bf16),
+            pltpu.VMEM((per_core, 3, slab, strip), bf16),
+            pltpu.VMEM((per_core, slab, strip), bf16),
+            pltpu.VMEM((per_core, slab, strip), bf16),
             pltpu.VMEM((rows + 8, 256), f32),
             pltpu.VMEM(((GROUP + 1) * EDGE, width), bf16),
             pltpu.VMEM((blocks, GROUP * EDGE, 256), f32),
@@ -943,7 +1056,7 @@
             pltpu.VMEM((piece, local), f32),
             pltpu.VMEM((piece, local), f32),
             pltpu.VMEM((local, out_piece), f32),
-            pltpu.VMEM((blocks + 4, rows, 256), f32),
+            pltpu.VMEM((blocks + 2, rows, 256), f32),
             pltpu.VMEM((1, width), f32),
             pltpu.VMEM((local // 128, 128), f32),
             pltpu.VMEM((local // 128, 128), f32),
@@ -978,6 +1091,12 @@
             dma((per_core,)),
             dma((1,)),
             dma((per_core, 2)),
+            dma((1,)),
+            dma((per_core,)),
+            dma((1,)),
+            dma((per_core,)),
+            dma((1,)),
+            dma((per_core,)),
         ],
         compiler_params=pltpu.CompilerParams(
             collective_id=0, has_side_effects=True, vmem_limit_bytes=65400000

time: 152 us -> 150 us (0.987)
  Pallas kernels: 151 us -> 149 us
    pallas_call x1, Pallas kernels: 151 us -> 149 us  [grouped_body(): pl.pallas_call(functools.partial(fused_kernel, planes), out_shape=pltpu.V...]
where the time goes in v5:
time: 150 us
  Pallas kernels  149 us (99%)
    pallas_call x1, Pallas kernels, grouped_body(): pl.pallas_call(functools.partial(fused_kernel, planes), out_shape=pltpu.V...  149 us

profile of v5, /device:TPU:1, one launch (start us, length us, event | category | flops | bytes accessed | tf_op | source)
XLA Modules:
  0.0 150.0 jit_solution(18159637949368605916)
XLA Ops:
  0.0 148.8 %shard_map.118 = bf16[768,1024]{1,0:T(8,128)(2,1)S(1)} custom-call(bf16[768,2048]{1,0:T(8,128)(2,1)} %tok_hbm.1, f32[128,2560]{1,0:T(8,128)} %gate_hbm.1, f32[128,2560]{1,0:T(8,128)} %value_hbm.1, f32[2560,128]{1,0:T(8,128)} %down_hbm.1, f32[1,2048]{1,0:T(1,128)} %bitcast.10, f32[20,128]{1,0:T(8,128)} %bitcast.6, f32[20,128]{1,0:T(8,128)} %bitcast.7, ...), custom_call_target="tpu_custom_call" | custom-call | tf_op jit(solution)/shard_map/pallas_call | solution.py:1032
  148.9 1.1 copy.14

commit v6 on v5

--- a/solution.py
+++ b/solution.py
@@ -1024,7 +1024,7 @@
     strip = 2 * out_piece
     strips = chunk // strip
     per_core = half * strips
-    slab = max(1, rows // 8 // 32) * 32
+    slab = max(1, rows // 6 // 32) * 32
     dma = pltpu.SemaphoreType.DMA
     bf16, f32 = jnp.bfloat16, jnp.float32
     vmem = pl.BlockSpec(memory_space=pltpu.VMEM)

time: 150 us -> 150 us (level)
  no operation moved by 1% of the time
where the time goes in v6:
time: 150 us; the launch traced here: 149 us
  Pallas kernels  148 us (99%)
    pallas_call x1, Pallas kernels, grouped_body(): pl.pallas_call(functools.partial(fused_kernel, planes), out_shape=pltpu.V...  148 us

profile of v6, /device:TPU:1, one launch (start us, length us, event | category | flops | bytes accessed | tf_op | source)
XLA Modules:
  0.0 149.4 jit_solution(11171511520121645157)
XLA Ops:
  0.0 148.2 %shard_map.118 = bf16[768,1024]{1,0:T(8,128)(2,1)S(1)} custom-call(bf16[768,2048]{1,0:T(8,128)(2,1)} %tok_hbm.1, f32[128,2560]{1,0:T(8,128)} %gate_hbm.1, f32[128,2560]{1,0:T(8,128)} %value_hbm.1, f32[2560,128]{1,0:T(8,128)} %down_hbm.1, f32[1,2048]{1,0:T(1,128)} %bitcast.10, f32[20,128]{1,0:T(8,128)} %bitcast.6, f32[20,128]{1,0:T(8,128)} %bitcast.7, ...), custom_call_target="tpu_custom_call" | custom-call | tf_op jit(solution)/shard_map/pallas_call | solution.py:1032
  148.2 1.1 copy.14
